TPU v7x, 768 devices: a whole 4x8x12 slice. The times are simulated.
768 devices in a mesh: sp: 96 (over z, y), tp: 8 (over x, core).
Axes of the slice: x: 4, y: 8, z: 12, core: 2. Of those that a mesh axis runs over, the one named last changes fastest.
Arguments:
- tokens: bfloat16 [12288, 2048], P(('sp', 'tp')), may hold values from -70 to 70
- w_query: bfloat16 [2048, 2048], P(None, 'tp'), may hold values from -0.1875 to 0.1875
- w_key: bfloat16 [2048, 1024], P(None, 'tp'), may hold values from -0.1875 to 0.1875
- w_value: bfloat16 [2048, 1024], P(None, 'tp'), may hold values from -0.125 to 0.125
- w_out: bfloat16 [2048, 2048], P('tp'), may hold values from -0.125 to 0.125
- lambda_head: float32 [16], P('tp'), may hold values from 0.3 to 0.8
- sub_gain: float32 [128], replicated, may hold values from 0.1 to 1.9
Outputs:
- mixed_rows: bfloat16 [12288, 2048], P(('sp', 'tp'))
All inputs are finite; a program needn't handle non-finite values.
Results may differ from a plain program's by a relative error of at most 0.015.
The roundings to bfloat16 on the way count: a program that leaves them out, or rounds other values in their place, can miss the bound.
Values may be sent and summed in bfloat16 or wider, within the bound.
No kernel may reach another device: no remote copies, remote signals or barrier semaphores. Data moves between devices by JAX's collectives and lax.ppermute only.
A program may use at most 64 MiB of HBM per device.

v0:
```python
import math

import jax
import jax.numpy as jnp
from jax import lax
from jax.sharding import PartitionSpec as P

QK = 64
VD = 128


def joined_along(parts, dim):
    dims = list(parts.shape[1:])
    dims[dim] *= parts.shape[0]
    return jnp.moveaxis(parts, 0, dim).reshape(dims)


def from_everyone(value, axis):
    length = lax.axis_size(axis)
    return lax.all_to_all(
        jnp.broadcast_to(value[None], (length, *value.shape)), axis, 0, 0, tiled=True
    )


def gather_directly(value, axis, dim):
    return joined_along(from_everyone(value, axis), dim)


def in_one_piece(arrays, axis, dim, along):
    both = jnp.concatenate(arrays, axis=along)
    filled, at, done = (lax.all_gather(both, axis, axis=dim, tiled=True), 0, [])
    for a in arrays:
        done.append(lax.slice_in_dim(filled, at, at + a.shape[along], axis=along))
        at += a.shape[along]
    return tuple(done)


def split_up(value, dim, length):
    dims = value.shape
    parts = value.reshape(*dims[:dim], length, dims[dim] // length, *dims[dim + 1 :])
    return jnp.moveaxis(parts, dim, 0)


def summed_on_arrival(value, axis, dim):
    parts = split_up(value, dim, lax.axis_size(axis))
    arrived = lax.all_to_all(parts, axis, split_axis=0, concat_axis=0, tiled=True)
    return arrived.astype(jnp.float32).sum(axis=0)


def block_span(count_rows, unit_rows):
    chosen = unit_rows
    shard_total = count_rows // unit_rows
    for shards in range(1, 9):
        if shard_total % shards == 0 and shards * unit_rows <= 1024:
            chosen = shards * unit_rows
    return chosen


def body(tokens, w_query, w_key, w_value, w_out, lambda_head, sub_gain):
    query_cols = w_query.shape[1]
    key_cols = w_key.shape[1]
    group_count = key_cols // (2 * QK)
    joined = jnp.concatenate([w_query, w_key, w_value], axis=1)
    projected = jnp.dot(
        gather_directly(tokens, "tp", 0), joined, preferred_element_type=jnp.float32
    ).astype(jnp.bfloat16)
    row_count = projected.shape[0]
    queries = projected[:, :query_cols].reshape(row_count, group_count, 2, 2, QK)
    keys = projected[:, query_cols : query_cols + key_cols]
    values = projected[:, query_cols + key_cols :]
    first_row = lax.axis_index("sp") * row_count
    last_row = first_row + row_count - 1
    query_pos = first_row + jnp.arange(row_count, dtype=jnp.int32)
    score_scale = 1.0 / math.sqrt(QK)

    def absorb(running, key_block, value_block, block_start):
        row_peak, row_total, weighted = running
        span_rows = key_block.shape[0]
        shaped_keys = key_block.reshape(span_rows, group_count, 2, QK)
        shaped_values = value_block.reshape(span_rows, group_count, VD)
        scores = (
            jnp.einsum(
                "tkgmd,skmd->kgmts", queries, shaped_keys, preferred_element_type=jnp.float32
            )
            * score_scale
        )
        key_pos = block_start + jnp.arange(span_rows, dtype=jnp.int32)
        allowed = (key_pos[None, :] <= query_pos[:, None]) & (key_pos[None, :] >= 0)
        scores = jnp.where(allowed, scores, -jnp.inf)
        new_peak = jnp.maximum(row_peak, jnp.max(scores, axis=-1))
        exponent = jnp.exp(scores - new_peak[..., None])
        fading = jnp.exp(row_peak - new_peak)
        row_total = row_total * fading + jnp.sum(exponent, axis=-1)
        contrib = jnp.einsum(
            "kgmts,ske->kgmte",
            exponent.astype(jnp.bfloat16),
            shaped_values,
            preferred_element_type=jnp.float32,
        )
        weighted = weighted * fading[..., None] + contrib
        return (new_peak, row_total, weighted)

    empty_peak = jnp.full((group_count, 2, 2, row_count), -1e30, jnp.float32)
    running = (
        empty_peak,
        jnp.zeros_like(empty_peak),
        jnp.zeros((group_count, 2, 2, row_count, VD), jnp.float32),
    )
    key_part, value_part = in_one_piece((keys, values), "sp", 0, 1)
    span_rows = block_span(key_part.shape[0], row_count)
    turn_count = key_part.shape[0] // span_rows

    def one_turn(turn_index, carried):
        offset_rows = turn_index * span_rows

        def absorb_block(state_in):
            return absorb(
                state_in,
                lax.dynamic_slice_in_dim(key_part, offset_rows, span_rows, 0),
                lax.dynamic_slice_in_dim(value_part, offset_rows, span_rows, 0),
                offset_rows,
            )

        def unchanged(state_in):
            return state_in

        return lax.cond(offset_rows <= last_row, absorb_block, unchanged, carried)

    running = lax.fori_loop(0, turn_count, one_turn, running)
    row_peak, row_total, weighted = running
    normalized = weighted / row_total[..., None]
    group_lambda = lambda_head.reshape(group_count, 2)[:, :, None, None]
    mixed_out = normalized[:, :, 0] - group_lambda * normalized[:, :, 1]
    inverse_rms = lax.rsqrt(jnp.mean(mixed_out * mixed_out, axis=-1, keepdims=True) + 1e-06)
    heads = (mixed_out * inverse_rms * sub_gain).astype(jnp.bfloat16)
    heads = jnp.transpose(heads, (2, 0, 1, 3)).reshape(row_count, group_count * 2 * VD)
    mixed_rows = summed_on_arrival(
        jnp.dot(heads, w_out, preferred_element_type=jnp.float32).astype(jnp.bfloat16), "tp", 0
    )
    return mixed_rows.astype(jnp.bfloat16)


def solution(mesh):
    return jax.shard_map(
        body,
        mesh=mesh,
        in_specs=(
            P(("sp", "tp"), None),
            P(None, "tp"),
            P(None, "tp"),
            P(None, "tp"),
            P("tp", None),
            P("tp"),
            P(),
        ),
        out_specs=P(("sp", "tp"), None),
        check_vma=False,
    )
```

profile of v0, /device:TPU:704, one launch (start us, length us, event | category | flops | bytes accessed | tf_op | source)
XLA Modules:
  0.0 229.0 jit_solution(5333431614092265340)
XLA Ops:
  7.5 14.5 %all_to_all.10 = bf16[8,16,2048]{2,1,0:T(8,128)(2,1)S(1)} all-to-all(bf16[8,16,2048]{2,1,0:T(8,128)(2,1)S(1)} %broadcast_in_dim.34), channel_id=1, replica_groups=mesh['sp'=96,'tp'=8] {'tp'}, dimensions={0} | all-to-all | bytes 1048576 | tf_op jit(solution)/shard_map/all_to_all | solution.py:20
  22.0 2.3 %fusion.21 = bf16[128,512]{0,1:T(8,128)(2,1)S(1)} fusion(bf16[128,2048]{1,0:T(8,128)(2,1)S(1)} %bitcast.67, bf16[2048,128]{1,0:T(8,128)(2,1)} %param.14, bf16[2048,128]{1,0:T(8,128)(2,1)} %param.13, bf16[2048,256]{1,0:T(8,128)(2,1)} %param.12), kind=kOutput, calls=%fused_computation.30 | convolution fusion | flops 274792448 | bytes 2752512 | tf_op jit(solution)/shard_map/dot_general | solution.py:64
  25.0 124.6 %all-gather.2.cloned.1.call-done = bf16[12288,256]{0,1:T(8,128)(2,1)} async-done(((bf16[128,256]{0,1:T(8,128)(2,1)}), bf16[12288,256]{0,1:T(8,128)(2,1)}) %all-gather.2.cloned.1.call-update) | async-done | bytes 6291472 | tf_op jit(solution)/shard_map/all_gather | solution.py:31
  149.5 6.2 %fusion.28 = (bf16[12288,128]{0,1:T(8,128)(2,1)}, bf16[12288,128]{0,1:T(8,128)(2,1)}) fusion(bf16[12288,256]{0,1:T(8,128)(2,1)} %all-gather.2.cloned.1.call-done), kind=kLoop, calls=%fused_computation.41 | loop fusion | bytes 12582912 | tf_op jit(solution)/shard_map/slice | solution.py:33
  155.7 4.7 %copy.17 = bf16[12288,128]{1,0:T(8,128)(2,1)} copy(bf16[12288,128]{0,1:T(8,128)(2,1)} %get-tuple-element.270) | data formatting | bytes 6291456
  160.4 45.9 %while.18 = (s32[]{:T(128)}, f32[1,2,2,128]{3,1,2,0:T(2,128)S(1)}, f32[1,2,2,128]{3,1,2,0:T(2,128)S(1)}, f32[1,2,2,128,128]{4,3,2,1,0:T(8,128)S(1)}, s32[]{:T(12...) while((s32[]{:T(128)}, f32[1,2,2,128]{3,1,2,0:T(2,128)S(1)}, ...), condition=%wide.region_5.6_spmd.clone, body=%wide.region_0.5_spmd.clone.sunk | while | flops 204870272 | bytes 8239421 | solution.py:129
  160.5 3.8 %conditional.3 = ((f32[1,2,2,128]{3,1,2,0:T(2,128)S(1)}, f32[1,2,2,128]{3,1,2,0:T(2,128)S(1)}, f32[1,2,2,128,128]{4,3,2,1,0:T(8,128)S(1)})) conditional(s32[]{:T(128)} %convert_element_type.46, (f32[1,2,2,128]{3,1,2,0:T(2,128)S(1)}, f32[1,2,2,128]{3,1,2,0:T(2,128)S(1)}, f32[1,2,2,128,128]{4,3,2,1,0:T(8,128)S(1)}) %tuple.49, (s32[]{:T(128)}, ...), branch_computations={%region_1.0_spmd, %region_2.4_spmd} | conditional | flops 204870272 | bytes 8238678 | solution.py:127
  162.7 1.5 fusion.4
  164.3 3.8 %conditional.3 = ((f32[1,2,2,128]{3,1,2,0:T(2,128)S(1)}, f32[1,2,2,128]{3,1,2,0:T(2,128)S(1)}, f32[1,2,2,128,128]{4,3,2,1,0:T(8,128)S(1)})) conditional(s32[]{:T(128)} %convert_element_type.46, (f32[1,2,2,128]{3,1,2,0:T(2,128)S(1)}, f32[1,2,2,128]{3,1,2,0:T(2,128)S(1)}, f32[1,2,2,128,128]{4,3,2,1,0:T(8,128)S(1)}) %tuple.49, (s32[]{:T(128)}, ...), branch_computations={%region_1.0_spmd, %region_2.4_spmd} | conditional | flops 204870272 | bytes 8238678 | solution.py:127
  166.6 1.5 fusion.4
  168.1 3.8 %conditional.3 = ((f32[1,2,2,128]{3,1,2,0:T(2,128)S(1)}, f32[1,2,2,128]{3,1,2,0:T(2,128)S(1)}, f32[1,2,2,128,128]{4,3,2,1,0:T(8,128)S(1)})) conditional(s32[]{:T(128)} %convert_element_type.46, (f32[1,2,2,128]{3,1,2,0:T(2,128)S(1)}, f32[1,2,2,128]{3,1,2,0:T(2,128)S(1)}, f32[1,2,2,128,128]{4,3,2,1,0:T(8,128)S(1)}) %tuple.49, (s32[]{:T(128)}, ...), branch_computations={%region_1.0_spmd, %region_2.4_spmd} | conditional | flops 204870272 | bytes 8238678 | solution.py:127
  171.9 3.8 %conditional.3 = ((f32[1,2,2,128]{3,1,2,0:T(2,128)S(1)}, f32[1,2,2,128]{3,1,2,0:T(2,128)S(1)}, f32[1,2,2,128,128]{4,3,2,1,0:T(8,128)S(1)})) conditional(s32[]{:T(128)} %convert_element_type.46, (f32[1,2,2,128]{3,1,2,0:T(2,128)S(1)}, f32[1,2,2,128]{3,1,2,0:T(2,128)S(1)}, f32[1,2,2,128,128]{4,3,2,1,0:T(8,128)S(1)}) %tuple.49, (s32[]{:T(128)}, ...), branch_computations={%region_1.0_spmd, %region_2.4_spmd} | conditional | flops 204870272 | bytes 8238678 | solution.py:127
  174.2 1.5 fusion.4
  175.8 3.8 %conditional.3 = ((f32[1,2,2,128]{3,1,2,0:T(2,128)S(1)}, f32[1,2,2,128]{3,1,2,0:T(2,128)S(1)}, f32[1,2,2,128,128]{4,3,2,1,0:T(8,128)S(1)})) conditional(s32[]{:T(128)} %convert_element_type.46, (f32[1,2,2,128]{3,1,2,0:T(2,128)S(1)}, f32[1,2,2,128]{3,1,2,0:T(2,128)S(1)}, f32[1,2,2,128,128]{4,3,2,1,0:T(8,128)S(1)}) %tuple.49, (s32[]{:T(128)}, ...), branch_computations={%region_1.0_spmd, %region_2.4_spmd} | conditional | flops 204870272 | bytes 8238678 | solution.py:127
  179.6 3.8 %conditional.3 = ((f32[1,2,2,128]{3,1,2,0:T(2,128)S(1)}, f32[1,2,2,128]{3,1,2,0:T(2,128)S(1)}, f32[1,2,2,128,128]{4,3,2,1,0:T(8,128)S(1)})) conditional(s32[]{:T(128)} %convert_element_type.46, (f32[1,2,2,128]{3,1,2,0:T(2,128)S(1)}, f32[1,2,2,128]{3,1,2,0:T(2,128)S(1)}, f32[1,2,2,128,128]{4,3,2,1,0:T(8,128)S(1)}) %tuple.49, (s32[]{:T(128)}, ...), branch_computations={%region_1.0_spmd, %region_2.4_spmd} | conditional | flops 204870272 | bytes 8238678 | solution.py:127
  181.9 1.5 fusion.4
  183.4 3.8 %conditional.3 = ((f32[1,2,2,128]{3,1,2,0:T(2,128)S(1)}, f32[1,2,2,128]{3,1,2,0:T(2,128)S(1)}, f32[1,2,2,128,128]{4,3,2,1,0:T(8,128)S(1)})) conditional(s32[]{:T(128)} %convert_element_type.46, (f32[1,2,2,128]{3,1,2,0:T(2,128)S(1)}, f32[1,2,2,128]{3,1,2,0:T(2,128)S(1)}, f32[1,2,2,128,128]{4,3,2,1,0:T(8,128)S(1)}) %tuple.49, (s32[]{:T(128)}, ...), branch_computations={%region_1.0_spmd, %region_2.4_spmd} | conditional | flops 204870272 | bytes 8238678 | solution.py:127
  187.2 3.8 %conditional.3 = ((f32[1,2,2,128]{3,1,2,0:T(2,128)S(1)}, f32[1,2,2,128]{3,1,2,0:T(2,128)S(1)}, f32[1,2,2,128,128]{4,3,2,1,0:T(8,128)S(1)})) conditional(s32[]{:T(128)} %convert_element_type.46, (f32[1,2,2,128]{3,1,2,0:T(2,128)S(1)}, f32[1,2,2,128]{3,1,2,0:T(2,128)S(1)}, f32[1,2,2,128,128]{4,3,2,1,0:T(8,128)S(1)}) %tuple.49, (s32[]{:T(128)}, ...), branch_computations={%region_1.0_spmd, %region_2.4_spmd} | conditional | flops 204870272 | bytes 8238678 | solution.py:127
  189.5 1.5 fusion.4
  191.1 3.8 %conditional.3 = ((f32[1,2,2,128]{3,1,2,0:T(2,128)S(1)}, f32[1,2,2,128]{3,1,2,0:T(2,128)S(1)}, f32[1,2,2,128,128]{4,3,2,1,0:T(8,128)S(1)})) conditional(s32[]{:T(128)} %convert_element_type.46, (f32[1,2,2,128]{3,1,2,0:T(2,128)S(1)}, f32[1,2,2,128]{3,1,2,0:T(2,128)S(1)}, f32[1,2,2,128,128]{4,3,2,1,0:T(8,128)S(1)}) %tuple.49, (s32[]{:T(128)}, ...), branch_computations={%region_1.0_spmd, %region_2.4_spmd} | conditional | flops 204870272 | bytes 8238678 | solution.py:127
  194.9 3.8 %conditional.3 = ((f32[1,2,2,128]{3,1,2,0:T(2,128)S(1)}, f32[1,2,2,128]{3,1,2,0:T(2,128)S(1)}, f32[1,2,2,128,128]{4,3,2,1,0:T(8,128)S(1)})) conditional(s32[]{:T(128)} %convert_element_type.46, (f32[1,2,2,128]{3,1,2,0:T(2,128)S(1)}, f32[1,2,2,128]{3,1,2,0:T(2,128)S(1)}, f32[1,2,2,128,128]{4,3,2,1,0:T(8,128)S(1)}) %tuple.49, (s32[]{:T(128)}, ...), branch_computations={%region_1.0_spmd, %region_2.4_spmd} | conditional | flops 204870272 | bytes 8238678 | solution.py:127
  198.7 3.8 %conditional.3 = ((f32[1,2,2,128]{3,1,2,0:T(2,128)S(1)}, f32[1,2,2,128]{3,1,2,0:T(2,128)S(1)}, f32[1,2,2,128,128]{4,3,2,1,0:T(8,128)S(1)})) conditional(s32[]{:T(128)} %convert_element_type.46, (f32[1,2,2,128]{3,1,2,0:T(2,128)S(1)}, f32[1,2,2,128]{3,1,2,0:T(2,128)S(1)}, f32[1,2,2,128,128]{4,3,2,1,0:T(8,128)S(1)}) %tuple.49, (s32[]{:T(128)}, ...), branch_computations={%region_1.0_spmd, %region_2.4_spmd} | conditional | flops 204870272 | bytes 8238678 | solution.py:127
  202.5 3.8 %conditional.3 = ((f32[1,2,2,128]{3,1,2,0:T(2,128)S(1)}, f32[1,2,2,128]{3,1,2,0:T(2,128)S(1)}, f32[1,2,2,128,128]{4,3,2,1,0:T(8,128)S(1)})) conditional(s32[]{:T(128)} %convert_element_type.46, (f32[1,2,2,128]{3,1,2,0:T(2,128)S(1)}, f32[1,2,2,128]{3,1,2,0:T(2,128)S(1)}, f32[1,2,2,128,128]{4,3,2,1,0:T(8,128)S(1)}) %tuple.49, (s32[]{:T(128)}, ...), branch_computations={%region_1.0_spmd, %region_2.4_spmd} | conditional | flops 204870272 | bytes 8238678 | solution.py:127
  207.1 14.4 %all_to_all.11 = bf16[8,16,2048]{2,1,0:T(8,128)(2,1)S(1)} all-to-all(bf16[8,16,2048]{2,1,0:T(8,128)(2,1)S(1)} %bitcast.65), channel_id=1, replica_groups=mesh['sp'=96,'tp'=8] {'tp'}, dimensions={0} | all-to-all | bytes 1048576 | tf_op jit(solution)/shard_map/all_to_all | solution.py:46
  (172 shorter events, 40.1 us)
Async XLA Ops:
  6.5 200.2 %copy-start = (bf16[256,2048]{1,0:T(8,128)(2,1)S(1)}, bf16[256,2048]{1,0:T(8,128)(2,1)}, u32[]{:S(2)}) copy-start(bf16[256,2048]{1,0:T(8,128)(2,1)} %param.15) | copy-start | bytes 3145732
  6.5 143.0 %all-gather.2.cloned.1.call-start = ((), (), s32[]{:S(2)}) async-start(), calls=%async_computation.2 | async-start | bytes 6356992 | tf_op jit(solution)/shard_map/all_gather | solution.py:31
  160.4 46.1 %copy-start.1 = (f32[2]{0:T(128)S(1)}, f32[2]{0:T(128)}, u32[]{:S(2)}) copy-start(f32[2]{0:T(128)} %param.16) | copy-start | bytes 28
  160.4 46.2 %copy-start.2 = (f32[128]{0:T(128)S(1)}, f32[128]{0:T(128)}, u32[]{:S(2)}) copy-start(f32[128]{0:T(128)} %param.17) | copy-start | bytes 1540
Sparse Core Ops, SparseCore 0:
  25.1 124.4 all-gather.1
where the time goes:
time: 230 us; the launch traced here: 229 us
  waiting for transfers between devices  125 us (54%)
  blocking collectives  28.9 us (13%)
  matrix products  26.4 us (11%)
  local copies, waits for them, and re-layouts  24.4 us (11%)
  between operations  13.5 us (6%)
  other arithmetic  9.85 us (4%)
    all_gather x1, waiting for transfers between devices, in_one_piece(): filled, at, done = (lax.all_gather(both, axis, axis=dim, tiled=True), 0, [])  125 us
    dot_general x12, matrix products, absorb(): jnp.einsum('kgmts,ske->kgmte', exponent.astype(jnp.bfloat16), shaped_valu...  17.7 us
    all_to_all x1, blocking collectives, from_everyone(): lax.all_to_all(jnp.broadcast_to(value[None], (length, *value.shape)), axi...  14.5 us
    all_to_all x1, blocking collectives, summed_on_arrival(): lax.all_to_all(parts, axis, split_axis=0, concat_axis=0, tiled=True)  14.4 us
    dynamic_slice x12, local copies, waits for them, and re-layouts, absorb_block(): lax.dynamic_slice_in_dim(key_part, offset_rows, span_rows, 0)  11.7 us
    slice x1, local copies, waits for them, and re-layouts, in_one_piece(): done.append(lax.slice_in_dim(filled, at, at + a.shape[along], axis=along))  6.17 us
    dot_general x12, matrix products, absorb(): jnp.einsum('tkgmd,skmd->kgmts', queries, shaped_keys, preferred_element_t...  6.03 us
    unnamed x8, local copies, waits for them, and re-layouts  4.67 us
  transfers between devices with their start and end apart: 1, of which 1 were waited for; matrix products, arithmetic and copies ran while one was open for 0% of the time, Pallas kernels for 0%

commit v1 on v0

v1 whole, which is shorter than its diff:
```python
import functools
import math

import jax
import jax.numpy as jnp
from jax import lax
from jax.experimental import pallas as pl
from jax.experimental.pallas import tpu as pltpu
from jax.sharding import Mesh, PartitionSpec as P

QK = 64
VD = 128
BLOCK = 128
Y = 8
STAT_ROWS = 16
SEND_ROWS = 2 * VD + STAT_ROWS
EMPTY = -1e30
HIDDEN = -2e38
BASE2_SCALE = math.log2(math.e) / math.sqrt(QK)

VMEM = pl.BlockSpec(memory_space=pltpu.VMEM)
SMEM = pl.BlockSpec(memory_space=pltpu.SMEM)


def three_parts(value):
    high = value.astype(jnp.bfloat16)
    rest = value - high.astype(jnp.float32)
    middle = rest.astype(jnp.bfloat16)
    low = (rest - middle.astype(jnp.float32)).astype(jnp.bfloat16)
    return [part.astype(jnp.float32) for part in (high, middle, low)]


def attend_block(row_blocks, place_ref, q_ref, kv_ref, out_ref, b):
    z, y = place_ref[0], place_ref[1]
    q_block = q_ref[b]
    q_rows = jnp.concatenate([q_block[:, : 2 * QK], q_block[:, 2 * QK :]], axis=0)
    lane = lax.broadcasted_iota(jnp.int32, q_rows.shape, 1)
    k_rows = jnp.concatenate([kv_ref[i, :BLOCK, :] for i in range(row_blocks)], axis=0)
    v_cols = jnp.concatenate([kv_ref[i, BLOCK:, :] for i in range(row_blocks)], axis=1)
    span = row_blocks * BLOCK
    masked = 4 * BLOCK
    r = lax.broadcasted_iota(jnp.int32, (masked, 2 * BLOCK), 0)
    c = lax.broadcasted_iota(jnp.int32, (masked, 2 * BLOCK), 1)
    key_pos = ((r // BLOCK + (row_blocks - 4)) * Y + y) * BLOCK + r % BLOCK
    query_pos = (z * Y + b) * BLOCK + c % BLOCK
    allowed = key_pos <= query_pos
    stats = []
    for m in range(2):
        q_map = jnp.where((lane >= QK) == (m == 1), q_rows, jnp.zeros_like(q_rows))
        scores = lax.dot_general(
            k_rows, q_map, (((1,), (1,)), ((), ())), preferred_element_type=jnp.float32
        )
        tail = jnp.where(allowed, scores[span - masked :], HIDDEN)
        if span > masked:
            scores = jnp.concatenate([scores[: span - masked], tail], axis=0)
        else:
            scores = tail
        peak = jnp.maximum(jnp.max(scores, axis=0, keepdims=True), EMPTY)
        expo = jnp.exp2((scores - peak) * BASE2_SCALE)
        total = jnp.sum(expo, axis=0, keepdims=True)
        summed = jnp.dot(
            v_cols, expo.astype(jnp.bfloat16), preferred_element_type=jnp.float32
        )
        inverse = jnp.where(total > 0.0, 1.0 / total, 0.0)
        out_ref[b, m * VD : (m + 1) * VD, :] = (summed * inverse).astype(jnp.bfloat16)
        stats += three_parts(peak) + three_parts(total)
    stats += [jnp.zeros_like(stats[0])] * (STAT_ROWS - len(stats))
    out_ref[b, 2 * VD :, :] = jnp.concatenate(stats, axis=0).astype(jnp.bfloat16)


def attend_kernel(place_ref, q_ref, kv_ref, out_ref):
    z = place_ref[0]
    rows = kv_ref.shape[0]
    for row_blocks in range(4, rows + 1, 4):

        @pl.when((z >= row_blocks - 4) & (z < row_blocks))
        def _():
            @pl.loop(0, Y)
            def _(b):
                attend_block(row_blocks, place_ref, q_ref, kv_ref, out_ref, b)


def attend(place, queries, key_values):
    return pl.pallas_call(
        attend_kernel,
        out_shape=jax.ShapeDtypeStruct((Y, SEND_ROWS, 2 * BLOCK), jnp.bfloat16),
        in_specs=[SMEM, VMEM, VMEM],
        out_specs=VMEM,
        cost_estimate=pl.CostEstimate(
            flops=4_000_000_000, bytes_accessed=3_000_000, transcendentals=6_000_000
        ),
        name="attend",
    )(place, queries, key_values)


def merge_kernel(part_ref, lambda_ref, gain_ref, w_ref, out_ref):
    stats = [part_ref[s, 2 * VD :, :].astype(jnp.float32) for s in range(Y)]
    mixed = None
    for m in range(2):
        at = 6 * m
        peaks = [s[at : at + 1] + s[at + 1 : at + 2] + s[at + 2 : at + 3] for s in stats]
        totals = [s[at + 3 : at + 4] + s[at + 4 : at + 5] + s[at + 5 : at + 6] for s in stats]
        top = functools.reduce(jnp.maximum, peaks)
        shares = [jnp.exp2((p - top) * BASE2_SCALE) * t for p, t in zip(peaks, totals)]
        inverse = 1.0 / sum(shares)
        normalized = sum(
            part_ref[s, m * VD : (m + 1) * VD, :].astype(jnp.float32) * (shares[s] * inverse)
            for s in range(Y)
        )
        if m == 0:
            mixed = normalized
        else:
            column = lax.broadcasted_iota(jnp.int32, (1, 2 * BLOCK), 1)
            head_lambda = jnp.where(column < BLOCK, lambda_ref[0], lambda_ref[1])
            mixed = mixed - head_lambda * normalized
    inverse_rms = lax.rsqrt(jnp.mean(mixed * mixed, axis=0, keepdims=True) + 1e-06)
    heads = mixed * inverse_rms * gain_ref[...]
    rows = jnp.concatenate([heads[:, :BLOCK].T, heads[:, BLOCK:].T], axis=1)
    out_ref[...] = jnp.dot(
        rows.astype(jnp.bfloat16), w_ref[...], preferred_element_type=jnp.float32
    ).astype(jnp.bfloat16)


def merge(parts, lambda_head, sub_gain, w_out):
    return pl.pallas_call(
        merge_kernel,
        out_shape=jax.ShapeDtypeStruct((BLOCK, w_out.shape[1]), jnp.bfloat16),
        in_specs=[VMEM, SMEM, VMEM, VMEM],
        out_specs=VMEM,
        name="merge",
    )(parts, lambda_head, sub_gain.reshape(VD, 1), w_out)


def to_everyone(value, axis):
    length = lax.axis_size(axis)
    return lax.all_to_all(
        jnp.broadcast_to(value[None], (length, *value.shape)), axis, 0, 0, tiled=True
    )


def body(tokens, w_query, w_key, w_value, w_out, lambda_head, sub_gain):
    tp = lax.axis_size("tp")
    rows = to_everyone(tokens, "tp").reshape(tp * tokens.shape[0], tokens.shape[1])
    dot = functools.partial(lax.dot_general, preferred_element_type=jnp.float32)
    queries = dot(rows, w_query, (((1,), (0,)), ((), ()))).astype(jnp.bfloat16)
    keys = dot(rows, w_key, (((1,), (0,)), ((), ()))).astype(jnp.bfloat16)
    values = dot(w_value, rows, (((0,), (1,)), ((), ()))).astype(jnp.bfloat16)
    all_queries = to_everyone(queries, "y")
    key_values = lax.all_gather(jnp.concatenate([keys, values], axis=0), "z")
    place = jnp.stack([lax.axis_index("z"), lax.axis_index("y")]).astype(jnp.int32)
    parts = attend(place, all_queries, key_values)
    parts = lax.all_to_all(parts, "y", 0, 0, tiled=True)
    partial_rows = merge(parts, lambda_head, sub_gain, w_out)
    arrived = lax.all_to_all(
        partial_rows.reshape(tp, -1, partial_rows.shape[1]), "tp", 0, 0, tiled=True
    )
    return arrived.astype(jnp.float32).sum(axis=0).astype(jnp.bfloat16)


def solution(mesh):
    sp, tp = mesh.devices.shape
    grid = Mesh(mesh.devices.reshape(sp // Y, Y, tp), ("z", "y", "tp"))
    everyone = ("z", "y", "tp")
    return jax.shard_map(
        body,
        mesh=grid,
        in_specs=(
            P(everyone, None),
            P(None, "tp"),
            P(None, "tp"),
            P(None, "tp"),
            P("tp", None),
            P("tp"),
            P(),
        ),
        out_specs=P(everyone, None),
        check_vma=False,
    )
```

time: 230 us -> 127 us (0.55)
  the two profiles are of different devices: /device:TPU:704 before, /device:TPU:1 now
where the time goes in v1:
time: 127 us; the launch traced here: 126 us
  blocking collectives  46.6 us (37%)
  waiting for transfers between devices  34.4 us (27%)
  starting transfers between devices  24.5 us (19%)
  Pallas kernels  13.3 us (10%)
  local copies, waits for them, and re-layouts  5.16 us (4%)
  other arithmetic  1.29 us (1%)
    all_gather x1, blocking collectives, body(): key_values = lax.all_gather(jnp.concatenate([keys, values], axis=0), 'z')  29.1 us
    all_to_all x1, waiting for transfers between devices, body(): parts = lax.all_to_all(parts, 'y', 0, 0, tiled=True)  25.6 us
    all_to_all x1, blocking collectives, body(): lax.all_to_all(partial_rows.reshape(tp, -1, partial_rows.shape[1]), 'tp',...  17.5 us
    all_to_all x2, starting transfers between devices, to_everyone(): lax.all_to_all(jnp.broadcast_to(value[None], (length, *value.shape)), axi...  17.5 us
    pallas_call x1, Pallas kernels, attend(): pl.pallas_call(attend_kernel, out_shape=jax.ShapeDtypeStruct((Y, SEND_ROW...  10.2 us
    all_to_all x2, waiting for transfers between devices, to_everyone(): lax.all_to_all(jnp.broadcast_to(value[None], (length, *value.shape)), axi...  8.81 us
    all_to_all x1, starting transfers between devices, body(): parts = lax.all_to_all(parts, 'y', 0, 0, tiled=True)  7.05 us
    pallas_call x1, Pallas kernels, merge(): pl.pallas_call(merge_kernel, out_shape=jax.ShapeDtypeStruct((BLOCK, w_out...  3.12 us
  transfers between devices with their start and end apart: 3, of which 2 were waited for; matrix products, arithmetic and copies ran while one was open for 2% of the time, Pallas kernels for 0%

profile of v1, /device:TPU:1, one launch (start us, length us, event | category | flops | bytes accessed | tf_op | source)
XLA Modules:
  0.0 126.3 jit_solution(1003824312105392686)
XLA Ops:
  0.0 0.0 copy-start
  0.0 1.8 %broadcast_in_dim.4 = bf16[8,16,2048]{2,1,0:T(8,128)(2,1)} broadcast(bf16[16,2048]{1,0:T(8,128)(2,1)} %param.7), dimensions={1,2} | broadcast | bytes 589824 | tf_op jit(solution)/shard_map/broadcast_in_dim | solution.py:137
  1.8 13.9 %all-to-all-start = ((bf16[8,16,2048]{2,1,0:T(8,128)(2,1)}), bf16[8,16,2048]{2,1,0:T(8,128)(2,1)S(1)}, u32[]{:S(2)}, u32[]{:S(2)}) async-start(bf16[8,16,2048]{2,1,0:T(8,128)(2,1)} %broadcast_in_dim.4), calls=%async_computation | async-start | bytes 1048576 | tf_op jit(solution)/shard_map/all_to_all | solution.py:136
  15.7 0.6 pad_add_fusion.place_ref
  16.2 8.8 %all-to-all-done = bf16[8,16,2048]{2,1,0:T(8,128)(2,1)S(1)} async-done(((bf16[8,16,2048]{2,1,0:T(8,128)(2,1)}), bf16[8,16,2048]{2,1,0:T(8,128)(2,1)S(1)}, u32[]{:S(2)}, u32[]{:S(2)}) %all-to-all-start) | async-done | bytes 524320 | tf_op jit(solution)/shard_map/all_to_all | solution.py:136
  25.0 0.0 copy-done
  25.0 0.3 convolution_convert_fusion
  25.3 0.0 copy-start.2
  25.4 0.8 broadcast_in_dim.5
  26.2 3.6 %all-to-all-start.1 = ((bf16[8,128,256]{2,1,0:T(8,128)(2,1)}), bf16[8,128,256]{2,1,0:T(8,128)(2,1)S(1)}, u32[]{:S(2)}, u32[]{:S(2)}) async-start(bf16[8,128,256]{2,1,0:T(8,128)(2,1)} %broadcast_in_dim.5), calls=%async_computation.1 | async-start | bytes 1048576 | tf_op jit(solution)/shard_map/all_to_all | solution.py:136
  29.8 0.0 copy-done.2
  29.8 0.3 convolution_convert_fusion.1
  30.2 0.3 convolution_convert_fusion.2
  30.5 29.1 %all-gather = bf16[3072,128]{1,0:T(8,128)(2,1)} all-gather(bf16[256,128]{1,0:T(8,128)(2,1)S(1)} %pad_maximum_fusion), channel_id=2, replica_groups=mesh['z'=12,'y'=8,'tp'=8] {'z'}, dimensions={0}, use_global_device_ids=true | all-gather | bytes 851968 | tf_op jit(solution)/shard_map/all_gather | solution.py:149
  59.6 0.0 all-to-all-done.1.q_ref
  59.6 0.8 copy-done.4
  60.4 10.2 %attend.1 = bf16[8,272,256]{2,1,0:T(8,128)(2,1)} custom-call(s32[2]{0:T(128)} %pad_add_fusion.place_ref, bf16[8,128,256]{2,1,0:T(8,128)(2,1)} %copy-done.4, bf16[12,256,128]{2,1,0:T(8,128)(2,1)} %bitcast.16), custom_call_target="tpu_custom_call" | custom-call | flops 4000000000 | bytes 3000000 | tf_op jit(solution)/shard_map/attend/pallas_call | solution.py:84
  70.6 7.1 %all-to-all-start.2 = ((bf16[8,272,256]{2,1,0:T(8,128)(2,1)}), bf16[8,272,256]{2,1,0:T(8,128)(2,1)S(1)}, u32[]{:S(2)}, u32[]{:S(2)}) async-start(bf16[8,272,256]{2,1,0:T(8,128)(2,1)} %attend.1), calls=%async_computation.2 | async-start | bytes 2228224 | tf_op jit(solution)/shard_map/all_to_all | solution.py:152
  77.6 0.7 copy.8.gain_ref
  78.4 25.6 %all-to-all-done.2.part_ref = bf16[8,272,256]{2,1,0:T(8,128)(2,1)S(1)} async-done(((bf16[8,272,256]{2,1,0:T(8,128)(2,1)}), bf16[8,272,256]{2,1,0:T(8,128)(2,1)S(1)}, u32[]{:S(2)}, u32[]{:S(2)}) %all-to-all-start.2) | async-done | bytes 1114144 | tf_op jit(solution)/shard_map/all_to_all | solution.py:152
  103.9 1.0 copy-done.1
  104.9 3.1 %merge.1 = bf16[128,2048]{1,0:T(8,128)(2,1)} custom-call(bf16[8,272,256]{2,1,0:T(8,128)(2,1)} %copy-done.1, f32[2]{0:T(128)} %lambda_ref.1, f32[128,1]{1,0:T(8,128)} %copy.8.gain_ref, bf16[256,2048]{1,0:T(8,128)(2,1)} %w_ref.1), custom_call_target="tpu_custom_call" | custom-call | tf_op jit(solution)/shard_map/merge/pallas_call | solution.py:125
  108.1 17.5 %all_to_all.20 = bf16[8,16,2048]{2,1,0:T(8,128)(2,1)S(1)} all-to-all(bf16[8,16,2048]{2,1,0:T(8,128)(2,1)} %bitcast.15), channel_id=1, replica_groups=mesh['z'=12,'y'=8,'tp'=8] {'tp'}, dimensions={0} | all-to-all | bytes 1048576 | tf_op jit(solution)/shard_map/all_to_all | solution.py:154
  125.6 0.7 reduce_sum.12
  (7 shorter events, 0.0 us)
Async XLA Ops:
  0.0 25.0 %copy-start = (bf16[2048,256]{1,0:T(8,128)(2,1)S(1)}, bf16[2048,256]{1,0:T(8,128)(2,1)}, u32[]{:S(2)}) copy-start(bf16[2048,256]{1,0:T(8,128)(2,1)} %param.8) | copy-start | bytes 3145732
  1.8 23.2 %all-to-all-start = ((bf16[8,16,2048]{2,1,0:T(8,128)(2,1)}), bf16[8,16,2048]{2,1,0:T(8,128)(2,1)S(1)}, u32[]{:S(2)}, u32[]{:S(2)}) async-start(bf16[8,16,2048]{2,1,0:T(8,128)(2,1)} %broadcast_in_dim.4), calls=%async_computation | async-start | bytes 1048576 | tf_op jit(solution)/shard_map/all_to_all | solution.py:136
  25.3 4.5 %copy-start.2 = (bf16[2048,128]{1,0:T(8,128)(2,1)S(1)}, bf16[2048,128]{1,0:T(8,128)(2,1)}, u32[]{:S(2)}) copy-start(bf16[2048,128]{1,0:T(8,128)(2,1)} %param.10) | copy-start | bytes 1572868
  26.2 4.0 %copy-start.3 = (bf16[2048,128]{1,0:T(8,128)(2,1)S(1)}, bf16[2048,128]{1,0:T(8,128)(2,1)}, u32[]{:S(2)}) copy-start(bf16[2048,128]{1,0:T(8,128)(2,1)} %param.9) | copy-start | bytes 1572868
  26.2 33.4 %all-to-all-start.1 = ((bf16[8,128,256]{2,1,0:T(8,128)(2,1)}), bf16[8,128,256]{2,1,0:T(8,128)(2,1)S(1)}, u32[]{:S(2)}, u32[]{:S(2)}) async-start(bf16[8,128,256]{2,1,0:T(8,128)(2,1)} %broadcast_in_dim.5), calls=%async_computation.1 | async-start | bytes 1048576 | tf_op jit(solution)/shard_map/all_to_all | solution.py:136
  59.6 0.8 copy-start.4
  70.6 7.1 %copy-start.5 = (f32[128]{0:T(128)S(1)}, f32[128]{0:T(128)}, u32[]{:S(2)}) copy-start(f32[128]{0:T(128)} %param.13) | copy-start | bytes 1540
  70.6 33.4 %all-to-all-start.2 = ((bf16[8,272,256]{2,1,0:T(8,128)(2,1)}), bf16[8,272,256]{2,1,0:T(8,128)(2,1)S(1)}, u32[]{:S(2)}, u32[]{:S(2)}) async-start(bf16[8,272,256]{2,1,0:T(8,128)(2,1)} %attend.1), calls=%async_computation.2 | async-start | bytes 2228224 | tf_op jit(solution)/shard_map/all_to_all | solution.py:152
  103.9 1.0 copy-start.1

commit v2 on v1

v2 whole, which is shorter than its diff:
```python
import functools
import math

import jax
import jax.numpy as jnp
from jax import lax
from jax.experimental import pallas as pl
from jax.experimental.pallas import tpu as pltpu
from jax.sharding import Mesh, PartitionSpec as P

QK = 64
VD = 128
BLOCK = 128
TILE = 2 * BLOCK
Y = 8
STAT_ROWS = 16
SEND_ROWS = 2 * VD + STAT_ROWS
EMPTY = -1e30
HIDDEN = -2e38
BASE2_SCALE = math.log2(math.e) / math.sqrt(QK)
CASES = ((0, 3, 4, 4), (4, 7, 8, 4), (8, 10, 11, 3), (11, 11, 12, 1))

VMEM = pl.BlockSpec(memory_space=pltpu.VMEM)
SMEM = pl.BlockSpec(memory_space=pltpu.SMEM)


def three_parts(value):
    high = value.astype(jnp.bfloat16)
    rest = value - high.astype(jnp.float32)
    middle = rest.astype(jnp.bfloat16)
    low = (rest - middle.astype(jnp.float32)).astype(jnp.bfloat16)
    return [part.astype(jnp.float32) for part in (high, middle, low)]


def folded(op, value):
    return op(value.reshape(value.shape[0] // 8, 8, value.shape[1]), axis=0)


def score_pass(blocks, tail, place, q_ref, k_refs, b, offsets, score_refs):
    z, y = place
    q_block = q_ref[b]
    q_rows = jnp.concatenate([q_block[:, : 2 * QK], q_block[:, 2 * QK :]], axis=0)
    q_scaled = q_rows.astype(jnp.float32) * BASE2_SCALE
    high = q_scaled.astype(jnp.bfloat16)
    low = (q_scaled - high.astype(jnp.float32)).astype(jnp.bfloat16)
    peaks = []
    for m in range(2):
        lanes = slice(m * QK, (m + 1) * QK)
        q_map = jnp.concatenate([high[:, lanes], low[:, lanes]], axis=1)
        scores = lax.dot_general(
            k_refs[m][: blocks * BLOCK, :],
            q_map,
            (((1,), (1,)), ((), ())),
            preferred_element_type=jnp.float32,
        )
        top = jnp.full((8, TILE), EMPTY, jnp.float32)
        for block in range(blocks):
            rows = slice(block * BLOCK, (block + 1) * BLOCK)
            part = scores[rows]
            if block >= blocks - tail:
                reach = (z - block) * (Y * BLOCK) + (b - y) * BLOCK
                part = jnp.where(offsets <= reach, part, HIDDEN)
            score_refs[m][rows, :] = part
            top = jnp.maximum(top, folded(jnp.max, part))
        peaks.append(jnp.max(top, axis=0, keepdims=True))
    return peaks


def value_pass(blocks, v_ref, out_ref, b, score_refs, weight_refs, peaks):
    stats = []
    for m in range(2):
        peak = peaks[m]
        running = jnp.zeros((8, TILE), jnp.float32)
        for block in range(blocks):
            rows = slice(block * BLOCK, (block + 1) * BLOCK)
            expo = jnp.exp2(score_refs[m][rows, :] - peak)
            running = running + folded(jnp.sum, expo)
            weight_refs[m][rows, :] = expo.astype(jnp.bfloat16)
        total = jnp.sum(running, axis=0, keepdims=True)
        summed = jnp.dot(
            v_ref[:, : blocks * BLOCK],
            weight_refs[m][: blocks * BLOCK, :],
            preferred_element_type=jnp.float32,
        )
        inverse = jnp.where(total > 0.0, 1.0 / total, 0.0)
        out_ref[b, m * VD : (m + 1) * VD, :] = (summed * inverse).astype(jnp.bfloat16)
        stats += three_parts(peak) + three_parts(total)
    stats += [jnp.zeros_like(stats[0])] * (STAT_ROWS - len(stats))
    out_ref[b, 2 * VD :, :] = jnp.concatenate(stats, axis=0).astype(jnp.bfloat16)


def attend_kernel(place_ref, q_ref, kv_ref, out_ref, v_ref, k0_ref, k1_ref, *scratch):
    z, y = place_ref[0], place_ref[1]
    for block in range(kv_ref.shape[0]):
        rows = slice(block * BLOCK, (block + 1) * BLOCK)
        v_ref[:, rows] = kv_ref[block, BLOCK:, :]
        k = kv_ref[block, :BLOCK, :]
        k0_ref[rows, :] = jnp.concatenate([k[:, :QK], k[:, :QK]], axis=1)
        k1_ref[rows, :] = jnp.concatenate([k[:, QK:], k[:, QK:]], axis=1)
    key_row = lax.broadcasted_iota(jnp.int32, (BLOCK, TILE), 0)
    query_row = lax.rem(lax.broadcasted_iota(jnp.int32, (BLOCK, TILE), 1), BLOCK)
    offsets = key_row - query_row
    scores = (scratch[0:2], scratch[2:4])
    weights = (scratch[4:6], scratch[6:8])
    for low, high, blocks, tail in CASES:

        @pl.when((z >= low) & (z <= high))
        def _():
            def score(b, slot):
                return score_pass(
                    blocks, tail, (z, y), q_ref, (k0_ref, k1_ref), b, offsets, scores[slot]
                )

            def value(b, slot, peaks):
                value_pass(blocks, v_ref, out_ref, b, scores[slot], weights[slot], peaks)

            def two(i, peaks, more=True):
                odd = score(2 * i + 1, 1)
                value(2 * i, 0, peaks)
                even = score(2 * i + 2, 0) if more else None
                value(2 * i + 1, 1, odd)
                return even

            last = Y // 2 - 1
            two(last, lax.fori_loop(0, last, two, score(0, 0)), False)


def attend(place, queries, key_values):
    span = key_values.shape[0] * BLOCK
    return pl.pallas_call(
        attend_kernel,
        out_shape=jax.ShapeDtypeStruct((Y, SEND_ROWS, TILE), jnp.bfloat16),
        in_specs=[SMEM, VMEM, VMEM],
        out_specs=VMEM,
        scratch_shapes=[pltpu.VMEM((VD, span), jnp.bfloat16)]
        + [pltpu.VMEM((span, 2 * QK), jnp.bfloat16)] * 2
        + [pltpu.VMEM((span, TILE), jnp.float32)] * 4
        + [pltpu.VMEM((span, TILE), jnp.bfloat16)] * 4,
        compiler_params=pltpu.CompilerParams(vmem_limit_bytes=20 * 2**20),
        cost_estimate=pl.CostEstimate(
            flops=4_000_000_000, bytes_accessed=3_000_000, transcendentals=6_000_000
        ),
        name="attend",
    )(place, queries, key_values)


def merge_kernel(part_ref, lambda_ref, gain_ref, w_ref, out_ref):
    stats = [part_ref[s, 2 * VD :, :].astype(jnp.float32) for s in range(Y)]
    both = []
    for m in range(2):
        at = 6 * m
        peaks = [s[at : at + 1] + s[at + 1 : at + 2] + s[at + 2 : at + 3] for s in stats]
        totals = [s[at + 3 : at + 4] + s[at + 4 : at + 5] + s[at + 5 : at + 6] for s in stats]
        top = functools.reduce(jnp.maximum, peaks)
        shares = [jnp.exp2(p - top) * t for p, t in zip(peaks, totals)]
        inverse = 1.0 / sum(shares)
        both.append(
            sum(
                part_ref[s, m * VD : (m + 1) * VD, :].astype(jnp.float32) * (shares[s] * inverse)
                for s in range(Y)
            )
        )
    column = lax.broadcasted_iota(jnp.int32, (1, TILE), 1)
    mixed = both[0] - jnp.where(column < BLOCK, lambda_ref[0], lambda_ref[1]) * both[1]
    inverse_rms = lax.rsqrt(jnp.mean(mixed * mixed, axis=0, keepdims=True) + 1e-06)
    heads = mixed * inverse_rms * gain_ref[...]
    rows = jnp.concatenate([heads[:, :BLOCK].T, heads[:, BLOCK:].T], axis=1)
    out_ref[...] = jnp.dot(
        rows.astype(jnp.bfloat16), w_ref[...], preferred_element_type=jnp.float32
    ).astype(jnp.bfloat16)


def merge(parts, lambda_head, sub_gain, w_out):
    return pl.pallas_call(
        merge_kernel,
        out_shape=jax.ShapeDtypeStruct((BLOCK, w_out.shape[1]), jnp.bfloat16),
        in_specs=[VMEM, SMEM, VMEM, VMEM],
        out_specs=VMEM,
        compiler_params=pltpu.CompilerParams(vmem_limit_bytes=12 * 2**20),
        cost_estimate=pl.CostEstimate(
            flops=1_000_000_000, bytes_accessed=3_000_000, transcendentals=8_000
        ),
        name="merge",
    )(parts, lambda_head, sub_gain.reshape(VD, 1), w_out)


def to_everyone(value, axis):
    length = lax.axis_size(axis)
    return lax.all_to_all(
        jnp.broadcast_to(value[None], (length, *value.shape)), axis, 0, 0, tiled=True
    )


def body(tokens, w_query, w_key, w_value, w_out, lambda_head, sub_gain):
    tp = lax.axis_size("tp")
    rows = lax.all_gather(tokens, "tp", axis=0, tiled=True)
    dot = functools.partial(lax.dot_general, preferred_element_type=jnp.float32)
    queries = dot(rows, w_query, (((1,), (0,)), ((), ()))).astype(jnp.bfloat16)
    keys = dot(rows, w_key, (((1,), (0,)), ((), ()))).astype(jnp.bfloat16)
    values = dot(w_value, rows, (((0,), (1,)), ((), ()))).astype(jnp.bfloat16)
    all_queries = to_everyone(queries, "y")
    key_values = lax.all_gather(jnp.concatenate([keys, values], axis=0), "z")
    place = jnp.stack([lax.axis_index("z"), lax.axis_index("y")]).astype(jnp.int32)
    parts = attend(place, all_queries, key_values)
    parts = lax.all_to_all(parts, "y", 0, 0, tiled=True)
    partial_rows = merge(parts, lambda_head, sub_gain, w_out)
    arrived = lax.all_to_all(
        partial_rows.reshape(tp, -1, partial_rows.shape[1]), "tp", 0, 0, tiled=True
    )
    return arrived.astype(jnp.float32).sum(axis=0).astype(jnp.bfloat16)


def solution(mesh):
    sp, tp = mesh.devices.shape
    grid = Mesh(mesh.devices.reshape(sp // Y, Y, tp), ("z", "y", "tp"))
    everyone = ("z", "y", "tp")
    return jax.shard_map(
        body,
        mesh=grid,
        in_specs=(
            P(everyone, None),
            P(None, "tp"),
            P(None, "tp"),
            P(None, "tp"),
            P("tp", None),
            P("tp"),
            P(),
        ),
        out_specs=P(everyone, None),
        check_vma=False,
    )
```

time: 127 us -> 115 us (0.906)
  blocking collectives: 46.6 us -> 68.2 us
  starting transfers between devices: 24.5 us -> 10.7 us
  waiting for transfers between devices: 34.4 us -> 26.3 us
  Pallas kernels: 13.3 us -> 7.03 us
  local copies, waits for them, and re-layouts: 5.16 us -> 0.96 us
    all_gather x0 -> x1, blocking collectives: none -> 23.7 us  [body(): rows = lax.all_gather(tokens, 'tp', axis=0, tiled=True)]
    all_to_all x2 -> x1, starting transfers between devices: 17.5 us -> 3.62 us  [to_everyone(): lax.all_to_all(jnp.broadcast_to(value[None], (length, *value.shape)), axi...]
    all_to_all x2 -> x1, waiting for transfers between devices: 8.81 us -> 0.01 us  [to_everyone(): lax.all_to_all(jnp.broadcast_to(value[None], (length, *value.shape)), axi...]
    pallas_call x1, Pallas kernels: 10.2 us -> 5.81 us  [attend(): pl.pallas_call(attend_kernel, out_shape=jax.ShapeDtypeStruct((Y, SEND_ROW...]
    all_gather x1, blocking collectives: 29.1 us -> 26.9 us  [body(): key_values = lax.all_gather(jnp.concatenate([keys, values], axis=0), 'z')]
    pallas_call x1, Pallas kernels: 3.12 us -> 1.22 us  [merge(): pl.pallas_call(merge_kernel, out_shape=jax.ShapeDtypeStruct((BLOCK, w_out...]
    broadcast_in_dim x2 -> x1, local copies, waits for them, and re-layouts: 2.61 us -> 0.82 us  [to_everyone(): jnp.broadcast_to(value[None], (length, *value.shape))]
    unnamed x12, local copies, waits for them, and re-layouts: 1.81 us -> 0.03 us
  transfers between devices with their start and end apart: 3 -> 2, of which waited for: 2 -> 1; matrix products, arithmetic and copies ran while one was open for 2% -> 1% of each run, Pallas kernels for 0% -> 0%
where the time goes in v2:
time: 115 us
  blocking collectives  68.2 us (59%)
  waiting for transfers between devices  26.3 us (23%)
  starting transfers between devices  10.7 us (9%)
  Pallas kernels  7.03 us (6%)
    all_gather x1, blocking collectives, body(): key_values = lax.all_gather(jnp.concatenate([keys, values], axis=0), 'z')  26.9 us
    all_to_all x1, waiting for transfers between devices, body(): parts = lax.all_to_all(parts, 'y', 0, 0, tiled=True)  26.2 us
    all_gather x1, blocking collectives, body(): rows = lax.all_gather(tokens, 'tp', axis=0, tiled=True)  23.7 us
    all_to_all x1, blocking collectives, body(): lax.all_to_all(partial_rows.reshape(tp, -1, partial_rows.shape[1]), 'tp',...  17.6 us
    all_to_all x1, starting transfers between devices, body(): parts = lax.all_to_all(parts, 'y', 0, 0, tiled=True)  7.05 us
    pallas_call x1, Pallas kernels, attend(): pl.pallas_call(attend_kernel, out_shape=jax.ShapeDtypeStruct((Y, SEND_ROW...  5.81 us
    all_to_all x1, starting transfers between devices, to_everyone(): lax.all_to_all(jnp.broadcast_to(value[None], (length, *value.shape)), axi...  3.62 us
  transfers between devices with their start and end apart: 2, of which 1 were waited for; matrix products, arithmetic and copies ran while one was open for 1% of the time, Pallas kernels for 0%

profile of v2, /device:TPU:1, one launch (start us, length us, event | category | flops | bytes accessed | tf_op | source)
XLA Modules:
  0.0 115.0 jit_solution(6965794934058792924)
XLA Ops:
  0.0 0.0 copy-start
  0.0 23.7 %all_gather.9 = bf16[128,2048]{1,0:T(8,128)(2,1)S(1)} all-gather(bf16[16,2048]{1,0:T(8,128)(2,1)} %param.7), channel_id=1, replica_groups=mesh['z'=12,'y'=8,'tp'=8] {'tp'}, dimensions={0}, use_global_device_ids=true | all-gather | bytes 589824 | tf_op jit(solution)/shard_map/all_gather | solution.py:196
  23.8 0.0 copy-done
  23.8 0.3 convolution_convert_fusion
  24.1 0.0 copy-start.3
  24.1 0.8 broadcast_in_dim.2
  24.9 3.6 %all-to-all-start = ((bf16[8,128,256]{2,1,0:T(8,128)(2,1)}), bf16[8,128,256]{2,1,0:T(8,128)(2,1)S(1)}, u32[]{:S(2)}, u32[]{:S(2)}) async-start(bf16[8,128,256]{2,1,0:T(8,128)(2,1)} %broadcast_in_dim.2), calls=%async_computation | async-start | bytes 1048576 | tf_op jit(solution)/shard_map/all_to_all | solution.py:189
  28.6 0.1 pad_add_fusion.place_ref
  28.6 0.0 copy-done.3
  28.6 0.4 convolution_convert_fusion.1
  29.0 0.0 copy-done.4
  29.0 0.3 convolution_convert_fusion.2
  29.3 26.9 %all-gather = bf16[3072,128]{1,0:T(8,128)(2,1)S(1)} all-gather(bf16[256,128]{1,0:T(8,128)(2,1)S(1)} %pad_maximum_fusion), channel_id=2, replica_groups=mesh['z'=12,'y'=8,'tp'=8] {'z'}, dimensions={0}, use_global_device_ids=true | all-gather | bytes 851968 | tf_op jit(solution)/shard_map/all_gather | solution.py:202
  56.2 0.0 all-to-all-done.q_ref
  56.2 5.8 %attend.1 = bf16[8,272,256]{2,1,0:T(8,128)(2,1)} custom-call(s32[2]{0:T(128)S(1)} %pad_add_fusion.place_ref, bf16[8,128,256]{2,1,0:T(8,128)(2,1)S(1)} %all-to-all-done.q_ref, bf16[12,256,128]{2,1,0:T(8,128)(2,1)S(1)} %bitcast.11), custom_call_target="tpu_custom_call" | custom-call | flops 4000000000 | bytes 3000000 | tf_op jit(solution)/shard_map/attend/pallas_call | solution.py:130
  62.1 7.0 %all-to-all-start.1 = ((bf16[8,272,256]{2,1,0:T(8,128)(2,1)}), bf16[8,272,256]{2,1,0:T(8,128)(2,1)S(1)}, u32[]{:S(2)}, u32[]{:S(2)}) async-start(bf16[8,272,256]{2,1,0:T(8,128)(2,1)} %attend.1), calls=%async_computation.1 | async-start | bytes 2228224 | tf_op jit(solution)/shard_map/all_to_all | solution.py:205
  69.1 0.0 copy-done.5
  69.1 0.1 copy.8.gain_ref
  69.2 26.2 %all-to-all-done.1.part_ref = bf16[8,272,256]{2,1,0:T(8,128)(2,1)S(1)} async-done(((bf16[8,272,256]{2,1,0:T(8,128)(2,1)}), bf16[8,272,256]{2,1,0:T(8,128)(2,1)S(1)}, u32[]{:S(2)}, u32[]{:S(2)}) %all-to-all-start.1) | async-done | bytes 1114144 | tf_op jit(solution)/shard_map/all_to_all | solution.py:205
  95.5 0.0 copy-done.1
  95.5 0.0 copy-done.2
  95.5 1.2 %merge.1 = bf16[128,2048]{1,0:T(8,128)(2,1)S(1)} custom-call(bf16[8,272,256]{2,1,0:T(8,128)(2,1)S(1)} %all-to-all-done.1.part_ref, f32[2]{0:T(128)S(1)} %copy-done.2, f32[128,1]{1,0:T(8,128)S(1)} %copy.8.gain_ref, bf16[256,2048]{1,0:T(8,128)(2,1)S(1)} %copy-done.1), custom_call_target="tpu_custom_call" | custom-call | flops 1000000000 | bytes 3000000 | tf_op jit(solution)/shard_map/merge/pallas_call | solution.py:174
  96.7 17.6 %all_to_all.15 = bf16[8,16,2048]{2,1,0:T(8,128)(2,1)S(1)} all-to-all(bf16[8,16,2048]{2,1,0:T(8,128)(2,1)S(1)} %bitcast.12), channel_id=1, replica_groups=mesh['z'=12,'y'=8,'tp'=8] {'tp'}, dimensions={0} | all-to-all | bytes 1048576 | tf_op jit(solution)/shard_map/all_to_all | solution.py:207
  114.3 0.7 reduce_sum.12
  (5 shorter events, 0.0 us)
Async XLA Ops:
  0.0 23.8 %copy-start = (bf16[2048,256]{1,0:T(8,128)(2,1)S(1)}, bf16[2048,256]{1,0:T(8,128)(2,1)}, u32[]{:S(2)}) copy-start(bf16[2048,256]{1,0:T(8,128)(2,1)} %param.8) | copy-start | bytes 3145732
  24.1 4.6 %copy-start.3 = (bf16[2048,128]{1,0:T(8,128)(2,1)S(1)}, bf16[2048,128]{1,0:T(8,128)(2,1)}, u32[]{:S(2)}) copy-start(bf16[2048,128]{1,0:T(8,128)(2,1)} %param.10) | copy-start | bytes 1572868
  24.9 4.1 %copy-start.4 = (bf16[2048,128]{1,0:T(8,128)(2,1)S(1)}, bf16[2048,128]{1,0:T(8,128)(2,1)}, u32[]{:S(2)}) copy-start(bf16[2048,128]{1,0:T(8,128)(2,1)} %param.9) | copy-start | bytes 1572868
  24.9 31.3 %all-to-all-start = ((bf16[8,128,256]{2,1,0:T(8,128)(2,1)}), bf16[8,128,256]{2,1,0:T(8,128)(2,1)S(1)}, u32[]{:S(2)}, u32[]{:S(2)}) async-start(bf16[8,128,256]{2,1,0:T(8,128)(2,1)} %broadcast_in_dim.2), calls=%async_computation | async-start | bytes 1048576 | tf_op jit(solution)/shard_map/all_to_all | solution.py:189
  62.1 7.1 %copy-start.5 = (f32[128]{0:T(128)S(1)}, f32[128]{0:T(128)}, u32[]{:S(2)}) copy-start(f32[128]{0:T(128)} %param.13) | copy-start | bytes 1540
  62.1 33.4 %copy-start.1 = (bf16[256,2048]{1,0:T(8,128)(2,1)S(1)}, bf16[256,2048]{1,0:T(8,128)(2,1)}, u32[]{:S(2)}) copy-start(bf16[256,2048]{1,0:T(8,128)(2,1)} %w_ref.1) | copy-start | bytes 3145732
  62.1 33.4 %copy-start.2 = (f32[2]{0:T(128)S(1)}, f32[2]{0:T(128)}, u32[]{:S(2)}) copy-start(f32[2]{0:T(128)} %lambda_ref.1) | copy-start | bytes 28
  62.1 33.4 %all-to-all-start.1 = ((bf16[8,272,256]{2,1,0:T(8,128)(2,1)}), bf16[8,272,256]{2,1,0:T(8,128)(2,1)S(1)}, u32[]{:S(2)}, u32[]{:S(2)}) async-start(bf16[8,272,256]{2,1,0:T(8,128)(2,1)} %attend.1), calls=%async_computation.1 | async-start | bytes 2228224 | tf_op jit(solution)/shard_map/all_to_all | solution.py:205

commit v3 on v2

--- a/solution.py
+++ b/solution.py
@@ -18,7 +18,8 @@
 EMPTY = -1e30
 HIDDEN = -2e38
 BASE2_SCALE = math.log2(math.e) / math.sqrt(QK)
-CASES = ((0, 3, 4, 4), (4, 7, 8, 4), (8, 10, 11, 3), (11, 11, 12, 1))
+CASES = ((0, 0, 1), (1, 1, 2), (2, 2, 3), (3, 4, 5), (5, 7, 8), (8, 10, 11), (11, 11, 12))
+CHUNK = 2
 
 VMEM = pl.BlockSpec(memory_space=pltpu.VMEM)
 SMEM = pl.BlockSpec(memory_space=pltpu.SMEM)
@@ -36,93 +37,88 @@
     return op(value.reshape(value.shape[0] // 8, 8, value.shape[1]), axis=0)
 
 
-def score_pass(blocks, tail, place, q_ref, k_refs, b, offsets, score_refs):
-    z, y = place
+def both_maps(q_ref, b):
     q_block = q_ref[b]
     q_rows = jnp.concatenate([q_block[:, : 2 * QK], q_block[:, 2 * QK :]], axis=0)
     q_scaled = q_rows.astype(jnp.float32) * BASE2_SCALE
     high = q_scaled.astype(jnp.bfloat16)
     low = (q_scaled - high.astype(jnp.float32)).astype(jnp.bfloat16)
-    peaks = []
-    for m in range(2):
-        lanes = slice(m * QK, (m + 1) * QK)
-        q_map = jnp.concatenate([high[:, lanes], low[:, lanes]], axis=1)
-        scores = lax.dot_general(
-            k_refs[m][: blocks * BLOCK, :],
-            q_map,
-            (((1,), (1,)), ((), ())),
-            preferred_element_type=jnp.float32,
-        )
-        top = jnp.full((8, TILE), EMPTY, jnp.float32)
-        for block in range(blocks):
-            rows = slice(block * BLOCK, (block + 1) * BLOCK)
-            part = scores[rows]
-            if block >= blocks - tail:
-                reach = (z - block) * (Y * BLOCK) + (b - y) * BLOCK
-                part = jnp.where(offsets <= reach, part, HIDDEN)
-            score_refs[m][rows, :] = part
-            top = jnp.maximum(top, folded(jnp.max, part))
-        peaks.append(jnp.max(top, axis=0, keepdims=True))
-    return peaks
-
-
-def value_pass(blocks, v_ref, out_ref, b, score_refs, weight_refs, peaks):
-    stats = []
-    for m in range(2):
-        peak = peaks[m]
-        running = jnp.zeros((8, TILE), jnp.float32)
-        for block in range(blocks):
-            rows = slice(block * BLOCK, (block + 1) * BLOCK)
-            expo = jnp.exp2(score_refs[m][rows, :] - peak)
-            running = running + folded(jnp.sum, expo)
-            weight_refs[m][rows, :] = expo.astype(jnp.bfloat16)
-        total = jnp.sum(running, axis=0, keepdims=True)
-        summed = jnp.dot(
-            v_ref[:, : blocks * BLOCK],
-            weight_refs[m][: blocks * BLOCK, :],
-            preferred_element_type=jnp.float32,
-        )
-        inverse = jnp.where(total > 0.0, 1.0 / total, 0.0)
-        out_ref[b, m * VD : (m + 1) * VD, :] = (summed * inverse).astype(jnp.bfloat16)
-        stats += three_parts(peak) + three_parts(total)
-    stats += [jnp.zeros_like(stats[0])] * (STAT_ROWS - len(stats))
-    out_ref[b, 2 * VD :, :] = jnp.concatenate(stats, axis=0).astype(jnp.bfloat16)
+    return [
+        jnp.concatenate([high[:, m * QK : (m + 1) * QK], low[:, m * QK : (m + 1) * QK]], axis=1)
+        for m in range(2)
+    ]
 
 
 def attend_kernel(place_ref, q_ref, kv_ref, out_ref, v_ref, k0_ref, k1_ref, *scratch):
     z, y = place_ref[0], place_ref[1]
-    for block in range(kv_ref.shape[0]):
-        rows = slice(block * BLOCK, (block + 1) * BLOCK)
-        v_ref[:, rows] = kv_ref[block, BLOCK:, :]
-        k = kv_ref[block, :BLOCK, :]
-        k0_ref[rows, :] = jnp.concatenate([k[:, :QK], k[:, :QK]], axis=1)
-        k1_ref[rows, :] = jnp.concatenate([k[:, QK:], k[:, QK:]], axis=1)
+    k_refs = (k0_ref, k1_ref)
+    slots = (scratch[0:2], scratch[2:4])
     key_row = lax.broadcasted_iota(jnp.int32, (BLOCK, TILE), 0)
     query_row = lax.rem(lax.broadcasted_iota(jnp.int32, (BLOCK, TILE), 1), BLOCK)
     offsets = key_row - query_row
-    scores = (scratch[0:2], scratch[2:4])
-    weights = (scratch[4:6], scratch[6:8])
-    for low, high, blocks, tail in CASES:
-
-        @pl.when((z >= low) & (z <= high))
+
+    def step(case, later, slot_later, now, slot_now, peaks):
+        low, _, blocks = case
+        if later is not None:
+            queries = both_maps(q_ref, later)
+            tops = [jnp.full((8, TILE), EMPTY, jnp.float32) for _ in range(2)]
+        if now is not None:
+            totals = [jnp.zeros((8, TILE), jnp.float32) for _ in range(2)]
+            summed = [0.0, 0.0]
+        for first in range(0, blocks, CHUNK):
+            last = min(first + CHUNK, blocks)
+            rows = slice(first * BLOCK, last * BLOCK)
+            for m in range(2):
+                if later is not None:
+                    scores = lax.dot_general(
+                        k_refs[m][rows, :],
+                        queries[m],
+                        (((1,), (1,)), ((), ())),
+                        preferred_element_type=jnp.float32,
+                    )
+                    for block in range(first, last):
+                        part = scores[(block - first) * BLOCK : (block - first + 1) * BLOCK]
+                        if block >= low:
+                            reach = (z - block) * (Y * BLOCK) + (later - y) * BLOCK
+                            part = jnp.where(offsets <= reach, part, HIDDEN)
+                        slots[slot_later][m][block * BLOCK : (block + 1) * BLOCK, :] = part
+                        tops[m] = jnp.maximum(tops[m], folded(jnp.max, part))
+                if now is not None:
+                    expo = jnp.exp2(slots[slot_now][m][rows, :] - peaks[m])
+                    totals[m] = totals[m] + folded(jnp.sum, expo)
+                    summed[m] = summed[m] + jnp.dot(
+                        v_ref[:, rows], expo.astype(jnp.bfloat16), preferred_element_type=jnp.float32
+                    )
+        if now is not None:
+            stats = []
+            for m in range(2):
+                total = jnp.sum(totals[m], axis=0, keepdims=True)
+                inverse = jnp.where(total > 0.0, 1.0 / total, 0.0)
+                out_ref[now, m * VD : (m + 1) * VD, :] = (summed[m] * inverse).astype(jnp.bfloat16)
+                stats += three_parts(peaks[m]) + three_parts(total)
+            stats += [jnp.zeros_like(stats[0])] * (STAT_ROWS - len(stats))
+            out_ref[now, 2 * VD :, :] = jnp.concatenate(stats, axis=0).astype(jnp.bfloat16)
+        if later is not None:
+            return [jnp.max(top, axis=0, keepdims=True) for top in tops]
+        return None
+
+    for case in CASES:
+
+        @pl.when((z >= case[0]) & (z <= case[1]))
         def _():
-            def score(b, slot):
-                return score_pass(
-                    blocks, tail, (z, y), q_ref, (k0_ref, k1_ref), b, offsets, scores[slot]
-                )
-
-            def value(b, slot, peaks):
-                value_pass(blocks, v_ref, out_ref, b, scores[slot], weights[slot], peaks)
+            for block in range(case[2]):
+                rows = slice(block * BLOCK, (block + 1) * BLOCK)
+                v_ref[:, rows] = kv_ref[block, BLOCK:, :]
+                k = kv_ref[block, :BLOCK, :]
+                k0_ref[rows, :] = jnp.concatenate([k[:, :QK], k[:, :QK]], axis=1)
+                k1_ref[rows, :] = jnp.concatenate([k[:, QK:], k[:, QK:]], axis=1)
 
             def two(i, peaks, more=True):
-                odd = score(2 * i + 1, 1)
-                value(2 * i, 0, peaks)
-                even = score(2 * i + 2, 0) if more else None
-                value(2 * i + 1, 1, odd)
-                return even
-
-            last = Y // 2 - 1
-            two(last, lax.fori_loop(0, last, two, score(0, 0)), False)
+                odd = step(case, 2 * i + 1, 1, 2 * i, 0, peaks)
+                return step(case, 2 * i + 2 if more else None, 0, 2 * i + 1, 1, odd)
+
+            end = Y // 2 - 1
+            two(end, lax.fori_loop(0, end, two, step(case, 0, 0, None, 1, None)), False)
 
 
 def attend(place, queries, key_values):
@@ -134,9 +130,8 @@
         out_specs=VMEM,
         scratch_shapes=[pltpu.VMEM((VD, span), jnp.bfloat16)]
         + [pltpu.VMEM((span, 2 * QK), jnp.bfloat16)] * 2
-        + [pltpu.VMEM((span, TILE), jnp.float32)] * 4
-        + [pltpu.VMEM((span, TILE), jnp.bfloat16)] * 4,
-        compiler_params=pltpu.CompilerParams(vmem_limit_bytes=20 * 2**20),
+        + [pltpu.VMEM((span, TILE), jnp.float32)] * 4,
+        compiler_params=pltpu.CompilerParams(vmem_limit_bytes=16 * 2**20),
         cost_estimate=pl.CostEstimate(
             flops=4_000_000_000, bytes_accessed=3_000_000, transcendentals=6_000_000
         ),

time: 115 us -> 113 us (0.983)
  Pallas kernels: 7.03 us -> 5.2 us
    pallas_call x1, Pallas kernels: 5.81 us -> 3.99 us  [attend(): pl.pallas_call(attend_kernel, out_shape=jax.ShapeDtypeStruct((Y, SEND_ROW...]
where the time goes in v3:
time: 113 us
  blocking collectives  68.2 us (60%)
  waiting for transfers between devices  26.3 us (23%)
  starting transfers between devices  10.7 us (9%)
  Pallas kernels  5.2 us (5%)
    all_gather x1, blocking collectives, body(): key_values = lax.all_gather(jnp.concatenate([keys, values], axis=0), 'z')  26.9 us
    all_to_all x1, waiting for transfers between devices, body(): parts = lax.all_to_all(parts, 'y', 0, 0, tiled=True)  26.2 us
    all_gather x1, blocking collectives, body(): rows = lax.all_gather(tokens, 'tp', axis=0, tiled=True)  23.7 us
    all_to_all x1, blocking collectives, body(): lax.all_to_all(partial_rows.reshape(tp, -1, partial_rows.shape[1]), 'tp',...  17.6 us
    all_to_all x1, starting transfers between devices, body(): parts = lax.all_to_all(parts, 'y', 0, 0, tiled=True)  7.05 us
    pallas_call x1, Pallas kernels, attend(): pl.pallas_call(attend_kernel, out_shape=jax.ShapeDtypeStruct((Y, SEND_ROW...  3.99 us
    all_to_all x1, starting transfers between devices, to_everyone(): lax.all_to_all(jnp.broadcast_to(value[None], (length, *value.shape)), axi...  3.62 us
  transfers between devices with their start and end apart: 2, of which 1 were waited for; matrix products, arithmetic and copies ran while one was open for 1% of the time, Pallas kernels for 0%

profile of v3, /device:TPU:1, one launch (start us, length us, event | category | flops | bytes accessed | tf_op | source)
XLA Modules:
  0.0 113.2 jit_solution(2230956150145050558)
XLA Ops:
  0.0 0.0 copy-start
  0.0 23.7 %all_gather.9 = bf16[128,2048]{1,0:T(8,128)(2,1)S(1)} all-gather(bf16[16,2048]{1,0:T(8,128)(2,1)} %param.7), channel_id=1, replica_groups=mesh['z'=12,'y'=8,'tp'=8] {'tp'}, dimensions={0}, use_global_device_ids=true | all-gather | bytes 589824 | tf_op jit(solution)/shard_map/all_gather | solution.py:191
  23.8 0.0 copy-done
  23.8 0.3 convolution_convert_fusion
  24.1 0.0 copy-start.3
  24.1 0.8 broadcast_in_dim.2
  24.9 3.6 %all-to-all-start = ((bf16[8,128,256]{2,1,0:T(8,128)(2,1)}), bf16[8,128,256]{2,1,0:T(8,128)(2,1)S(1)}, u32[]{:S(2)}, u32[]{:S(2)}) async-start(bf16[8,128,256]{2,1,0:T(8,128)(2,1)} %broadcast_in_dim.2), calls=%async_computation | async-start | bytes 1048576 | tf_op jit(solution)/shard_map/all_to_all | solution.py:184
  28.6 0.1 pad_add_fusion.place_ref
  28.6 0.0 copy-done.3
  28.6 0.4 convolution_convert_fusion.1
  29.0 0.0 copy-done.4
  29.0 0.3 convolution_convert_fusion.2
  29.3 26.9 %all-gather = bf16[3072,128]{1,0:T(8,128)(2,1)S(1)} all-gather(bf16[256,128]{1,0:T(8,128)(2,1)S(1)} %pad_maximum_fusion), channel_id=2, replica_groups=mesh['z'=12,'y'=8,'tp'=8] {'z'}, dimensions={0}, use_global_device_ids=true | all-gather | bytes 851968 | tf_op jit(solution)/shard_map/all_gather | solution.py:197
  56.2 0.0 all-to-all-done.q_ref
  56.2 4.0 %attend.1 = bf16[8,272,256]{2,1,0:T(8,128)(2,1)} custom-call(s32[2]{0:T(128)S(1)} %pad_add_fusion.place_ref, bf16[8,128,256]{2,1,0:T(8,128)(2,1)S(1)} %all-to-all-done.q_ref, bf16[12,256,128]{2,1,0:T(8,128)(2,1)S(1)} %bitcast.11), custom_call_target="tpu_custom_call" | custom-call | flops 4000000000 | bytes 3000000 | tf_op jit(solution)/shard_map/attend/pallas_call | solution.py:126
  60.2 7.1 %all-to-all-start.1 = ((bf16[8,272,256]{2,1,0:T(8,128)(2,1)}), bf16[8,272,256]{2,1,0:T(8,128)(2,1)S(1)}, u32[]{:S(2)}, u32[]{:S(2)}) async-start(bf16[8,272,256]{2,1,0:T(8,128)(2,1)} %attend.1), calls=%async_computation.1 | async-start | bytes 2228224 | tf_op jit(solution)/shard_map/all_to_all | solution.py:200
  67.3 0.0 copy-done.5
  67.3 0.1 copy.8.gain_ref
  67.4 26.2 %all-to-all-done.1.part_ref = bf16[8,272,256]{2,1,0:T(8,128)(2,1)S(1)} async-done(((bf16[8,272,256]{2,1,0:T(8,128)(2,1)}), bf16[8,272,256]{2,1,0:T(8,128)(2,1)S(1)}, u32[]{:S(2)}, u32[]{:S(2)}) %all-to-all-start.1) | async-done | bytes 1114144 | tf_op jit(solution)/shard_map/all_to_all | solution.py:200
  93.7 0.0 copy-done.1
  93.7 0.0 copy-done.2
  93.7 1.2 %merge.1 = bf16[128,2048]{1,0:T(8,128)(2,1)S(1)} custom-call(bf16[8,272,256]{2,1,0:T(8,128)(2,1)S(1)} %all-to-all-done.1.part_ref, f32[2]{0:T(128)S(1)} %copy-done.2, f32[128,1]{1,0:T(8,128)S(1)} %copy.8.gain_ref, bf16[256,2048]{1,0:T(8,128)(2,1)S(1)} %copy-done.1), custom_call_target="tpu_custom_call" | custom-call | flops 1000000000 | bytes 3000000 | tf_op jit(solution)/shard_map/merge/pallas_call | solution.py:169
  94.9 17.6 %all_to_all.15 = bf16[8,16,2048]{2,1,0:T(8,128)(2,1)S(1)} all-to-all(bf16[8,16,2048]{2,1,0:T(8,128)(2,1)S(1)} %bitcast.12), channel_id=1, replica_groups=mesh['z'=12,'y'=8,'tp'=8] {'tp'}, dimensions={0} | all-to-all | bytes 1048576 | tf_op jit(solution)/shard_map/all_to_all | solution.py:202
  112.5 0.7 reduce_sum.12
  (5 shorter events, 0.0 us)
Async XLA Ops:
  0.0 23.8 %copy-start = (bf16[2048,256]{1,0:T(8,128)(2,1)S(1)}, bf16[2048,256]{1,0:T(8,128)(2,1)}, u32[]{:S(2)}) copy-start(bf16[2048,256]{1,0:T(8,128)(2,1)} %param.8) | copy-start | bytes 3145732
  24.1 4.6 %copy-start.3 = (bf16[2048,128]{1,0:T(8,128)(2,1)S(1)}, bf16[2048,128]{1,0:T(8,128)(2,1)}, u32[]{:S(2)}) copy-start(bf16[2048,128]{1,0:T(8,128)(2,1)} %param.10) | copy-start | bytes 1572868
  24.9 4.1 %copy-start.4 = (bf16[2048,128]{1,0:T(8,128)(2,1)S(1)}, bf16[2048,128]{1,0:T(8,128)(2,1)}, u32[]{:S(2)}) copy-start(bf16[2048,128]{1,0:T(8,128)(2,1)} %param.9) | copy-start | bytes 1572868
  24.9 31.3 %all-to-all-start = ((bf16[8,128,256]{2,1,0:T(8,128)(2,1)}), bf16[8,128,256]{2,1,0:T(8,128)(2,1)S(1)}, u32[]{:S(2)}, u32[]{:S(2)}) async-start(bf16[8,128,256]{2,1,0:T(8,128)(2,1)} %broadcast_in_dim.2), calls=%async_computation | async-start | bytes 1048576 | tf_op jit(solution)/shard_map/all_to_all | solution.py:184
  60.2 7.1 %copy-start.5 = (f32[128]{0:T(128)S(1)}, f32[128]{0:T(128)}, u32[]{:S(2)}) copy-start(f32[128]{0:T(128)} %param.13) | copy-start | bytes 1540
  60.2 33.4 %copy-start.1 = (bf16[256,2048]{1,0:T(8,128)(2,1)S(1)}, bf16[256,2048]{1,0:T(8,128)(2,1)}, u32[]{:S(2)}) copy-start(bf16[256,2048]{1,0:T(8,128)(2,1)} %w_ref.1) | copy-start | bytes 3145732
  60.2 33.4 %copy-start.2 = (f32[2]{0:T(128)S(1)}, f32[2]{0:T(128)}, u32[]{:S(2)}) copy-start(f32[2]{0:T(128)} %lambda_ref.1) | copy-start | bytes 28
  60.2 33.4 %all-to-all-start.1 = ((bf16[8,272,256]{2,1,0:T(8,128)(2,1)}), bf16[8,272,256]{2,1,0:T(8,128)(2,1)S(1)}, u32[]{:S(2)}, u32[]{:S(2)}) async-start(bf16[8,272,256]{2,1,0:T(8,128)(2,1)} %attend.1), calls=%async_computation.1 | async-start | bytes 2228224 | tf_op jit(solution)/shard_map/all_to_all | solution.py:200

commit v4 on v3

--- a/solution.py
+++ b/solution.py
@@ -13,7 +13,7 @@
 BLOCK = 128
 TILE = 2 * BLOCK
 Y = 8
-STAT_ROWS = 16
+STAT_ROWS = 8
 SEND_ROWS = 2 * VD + STAT_ROWS
 EMPTY = -1e30
 HIDDEN = -2e38
@@ -93,10 +93,10 @@
             stats = []
             for m in range(2):
                 total = jnp.sum(totals[m], axis=0, keepdims=True)
+                total = total.astype(jnp.bfloat16).astype(jnp.float32)
                 inverse = jnp.where(total > 0.0, 1.0 / total, 0.0)
                 out_ref[now, m * VD : (m + 1) * VD, :] = (summed[m] * inverse).astype(jnp.bfloat16)
-                stats += three_parts(peaks[m]) + three_parts(total)
-            stats += [jnp.zeros_like(stats[0])] * (STAT_ROWS - len(stats))
+                stats += three_parts(peaks[m]) + [total]
             out_ref[now, 2 * VD :, :] = jnp.concatenate(stats, axis=0).astype(jnp.bfloat16)
         if later is not None:
             return [jnp.max(top, axis=0, keepdims=True) for top in tops]
@@ -143,9 +143,9 @@
     stats = [part_ref[s, 2 * VD :, :].astype(jnp.float32) for s in range(Y)]
     both = []
     for m in range(2):
-        at = 6 * m
+        at = 4 * m
         peaks = [s[at : at + 1] + s[at + 1 : at + 2] + s[at + 2 : at + 3] for s in stats]
-        totals = [s[at + 3 : at + 4] + s[at + 4 : at + 5] + s[at + 5 : at + 6] for s in stats]
+        totals = [s[at + 3 : at + 4] for s in stats]
         top = functools.reduce(jnp.maximum, peaks)
         shares = [jnp.exp2(p - top) * t for p, t in zip(peaks, totals)]
         inverse = 1.0 / sum(shares)
@@ -158,8 +158,9 @@
     column = lax.broadcasted_iota(jnp.int32, (1, TILE), 1)
     mixed = both[0] - jnp.where(column < BLOCK, lambda_ref[0], lambda_ref[1]) * both[1]
     inverse_rms = lax.rsqrt(jnp.mean(mixed * mixed, axis=0, keepdims=True) + 1e-06)
-    heads = mixed * inverse_rms * gain_ref[...]
-    rows = jnp.concatenate([heads[:, :BLOCK].T, heads[:, BLOCK:].T], axis=1)
+    heads = mixed * inverse_rms
+    rows = [heads[:, h * BLOCK : (h + 1) * BLOCK].T * gain_ref[...] for h in range(2)]
+    rows = jnp.concatenate(rows, axis=1)
     out_ref[...] = jnp.dot(
         rows.astype(jnp.bfloat16), w_ref[...], preferred_element_type=jnp.float32
     ).astype(jnp.bfloat16)
@@ -176,7 +177,7 @@
             flops=1_000_000_000, bytes_accessed=3_000_000, transcendentals=8_000
         ),
         name="merge",
-    )(parts, lambda_head, sub_gain.reshape(VD, 1), w_out)
+    )(parts, lambda_head, sub_gain.reshape(1, VD), w_out)
 
 
 def to_everyone(value, axis):

time: 113 us -> 112 us (level)
  blocking collectives: 68.2 us -> 101 us
  waiting for transfers between devices: 26.3 us -> 0.01 us
  starting transfers between devices: 10.7 us -> 3.62 us
    all_to_all x0 -> x1, blocking collectives: none -> 30.6 us  [body(): parts = lax.all_to_all(parts, 'y', 0, 0, tiled=True)]
    all_to_all x1 -> x0, waiting for transfers between devices: 26.2 us -> none  [body(): parts = lax.all_to_all(parts, 'y', 0, 0, tiled=True)]
    all_to_all x1 -> x0, starting transfers between devices: 7.05 us -> none  [body(): parts = lax.all_to_all(parts, 'y', 0, 0, tiled=True)]
    all_to_all x1, blocking collectives: 17.6 us -> 19.5 us  [body(): lax.all_to_all(partial_rows.reshape(tp, -1, partial_rows.shape[1]), 'tp',...]
  transfers between devices with their start and end apart: 2 -> 1, of which waited for: 1 -> 0; matrix products, arithmetic and copies ran while one was open for 1% -> 1% of each run, Pallas kernels for 0% -> 0%
where the time goes in v4:
time: 112 us; the launch traced here: 111 us
  blocking collectives  101 us (90%)
  Pallas kernels  4.2 us (4%)
  starting transfers between devices  3.62 us (3%)
    all_to_all x1, blocking collectives, body(): parts = lax.all_to_all(parts, 'y', 0, 0, tiled=True)  30.6 us
    all_gather x1, blocking collectives, body(): key_values = lax.all_gather(jnp.concatenate([keys, values], axis=0), 'z')  26.9 us
    all_gather x1, blocking collectives, body(): rows = lax.all_gather(tokens, 'tp', axis=0, tiled=True)  23.7 us
    all_to_all x1, blocking collectives, body(): lax.all_to_all(partial_rows.reshape(tp, -1, partial_rows.shape[1]), 'tp',...  19.5 us
    all_to_all x1, starting transfers between devices, to_everyone(): lax.all_to_all(jnp.broadcast_to(value[None], (length, *value.shape)), axi...  3.62 us
    pallas_call x1, Pallas kernels, attend(): pl.pallas_call(attend_kernel, out_shape=jax.ShapeDtypeStruct((Y, SEND_ROW...  2.98 us
  transfers between devices with their start and end apart: 1, of which 0 were waited for; matrix products, arithmetic and copies ran while one was open for 1% of the time, Pallas kernels for 0%

profile of v4, /device:TPU:1, one launch (start us, length us, event | category | flops | bytes accessed | tf_op | source)
XLA Modules:
  0.0 111.2 jit_solution(18031940262800126589)
XLA Ops:
  0.0 0.0 copy-start
  0.0 23.7 %all_gather.9 = bf16[128,2048]{1,0:T(8,128)(2,1)S(1)} all-gather(bf16[16,2048]{1,0:T(8,128)(2,1)} %param.7), channel_id=1, replica_groups=mesh['z'=12,'y'=8,'tp'=8] {'tp'}, dimensions={0}, use_global_device_ids=true | all-gather | bytes 589824 | tf_op jit(solution)/shard_map/all_gather | solution.py:192
  23.8 0.0 copy-done
  23.8 0.3 convolution_convert_fusion
  24.1 0.0 copy-start.4
  24.1 0.8 broadcast_in_dim.2
  24.9 3.6 %all-to-all-start = ((bf16[8,128,256]{2,1,0:T(8,128)(2,1)}), bf16[8,128,256]{2,1,0:T(8,128)(2,1)S(1)}, u32[]{:S(2)}, u32[]{:S(2)}) async-start(bf16[8,128,256]{2,1,0:T(8,128)(2,1)} %broadcast_in_dim.2), calls=%async_computation | async-start | bytes 1048576 | tf_op jit(solution)/shard_map/all_to_all | solution.py:185
  28.5 0.1 pad_add_fusion.place_ref
  28.6 0.0 copy-done.4
  28.6 0.4 convolution_convert_fusion.1
  29.0 0.0 copy-done.5
  29.0 0.3 convolution_convert_fusion.2
  29.3 26.9 %all-gather = bf16[3072,128]{1,0:T(8,128)(2,1)S(1)} all-gather(bf16[256,128]{1,0:T(8,128)(2,1)S(1)} %pad_maximum_fusion), channel_id=2, replica_groups=mesh['z'=12,'y'=8,'tp'=8] {'z'}, dimensions={0}, use_global_device_ids=true | all-gather | bytes 851968 | tf_op jit(solution)/shard_map/all_gather | solution.py:198
  56.2 0.0 all-to-all-done.q_ref
  56.2 3.0 %attend.1 = bf16[8,264,256]{2,1,0:T(8,128)(2,1)S(1)} custom-call(s32[2]{0:T(128)S(1)} %pad_add_fusion.place_ref, bf16[8,128,256]{2,1,0:T(8,128)(2,1)S(1)} %all-to-all-done.q_ref, bf16[12,256,128]{2,1,0:T(8,128)(2,1)S(1)} %bitcast.11), custom_call_target="tpu_custom_call" | custom-call | flops 4000000000 | bytes 3000000 | tf_op jit(solution)/shard_map/attend/pallas_call | solution.py:126
  59.2 0.0 copy-start.1
  59.2 0.0 copy-start.2
  59.3 0.0 copy-start.3
  59.3 30.6 %all_to_all.15.part_ref = bf16[8,264,256]{2,1,0:T(8,128)(2,1)S(1)} all-to-all(bf16[8,264,256]{2,1,0:T(8,128)(2,1)S(1)} %attend.1), channel_id=1, replica_groups=mesh['z'=12,'y'=8,'tp'=8] {'y'}, dimensions={0} | all-to-all | bytes 2162688 | tf_op jit(solution)/shard_map/all_to_all | solution.py:201
  89.8 0.0 copy-done.1
  89.8 0.0 copy-done.2
  89.9 1.2 %merge.1 = bf16[128,2048]{1,0:T(8,128)(2,1)S(1)} custom-call(bf16[8,264,256]{2,1,0:T(8,128)(2,1)S(1)} %all_to_all.15.part_ref, f32[2]{0:T(128)S(1)} %copy-done.2, f32[1,128]{1,0:T(1,128)S(1)} %bitcast.13, bf16[256,2048]{1,0:T(8,128)(2,1)S(1)} %copy-done.1), custom_call_target="tpu_custom_call" | custom-call | flops 1000000000 | bytes 3000000 | tf_op jit(solution)/shard_map/merge/pallas_call | solution.py:170
  91.1 19.5 %all_to_all.16 = bf16[8,16,2048]{2,1,0:T(8,128)(2,1)S(1)} all-to-all(bf16[8,16,2048]{2,1,0:T(8,128)(2,1)S(1)} %bitcast.12), channel_id=1, replica_groups=mesh['z'=12,'y'=8,'tp'=8] {'tp'}, dimensions={0} | all-to-all | bytes 1048576 | tf_op jit(solution)/shard_map/all_to_all | solution.py:203
  110.5 0.7 reduce_sum.12
  (3 shorter events, 0.0 us)
Async XLA Ops:
  0.0 23.8 %copy-start = (bf16[2048,256]{1,0:T(8,128)(2,1)S(1)}, bf16[2048,256]{1,0:T(8,128)(2,1)}, u32[]{:S(2)}) copy-start(bf16[2048,256]{1,0:T(8,128)(2,1)} %param.8) | copy-start | bytes 3145732
  24.1 4.6 %copy-start.4 = (bf16[2048,128]{1,0:T(8,128)(2,1)S(1)}, bf16[2048,128]{1,0:T(8,128)(2,1)}, u32[]{:S(2)}) copy-start(bf16[2048,128]{1,0:T(8,128)(2,1)} %param.10) | copy-start | bytes 1572868
  24.9 4.1 %copy-start.5 = (bf16[2048,128]{1,0:T(8,128)(2,1)S(1)}, bf16[2048,128]{1,0:T(8,128)(2,1)}, u32[]{:S(2)}) copy-start(bf16[2048,128]{1,0:T(8,128)(2,1)} %param.9) | copy-start | bytes 1572868
  24.9 31.3 %all-to-all-start = ((bf16[8,128,256]{2,1,0:T(8,128)(2,1)}), bf16[8,128,256]{2,1,0:T(8,128)(2,1)S(1)}, u32[]{:S(2)}, u32[]{:S(2)}) async-start(bf16[8,128,256]{2,1,0:T(8,128)(2,1)} %broadcast_in_dim.2), calls=%async_computation | async-start | bytes 1048576 | tf_op jit(solution)/shard_map/all_to_all | solution.py:185
  59.2 30.6 %copy-start.1 = (bf16[256,2048]{1,0:T(8,128)(2,1)S(1)}, bf16[256,2048]{1,0:T(8,128)(2,1)}, u32[]{:S(2)}) copy-start(bf16[256,2048]{1,0:T(8,128)(2,1)} %w_ref.1) | copy-start | bytes 3145732
  59.2 30.6 %copy-start.2 = (f32[2]{0:T(128)S(1)}, f32[2]{0:T(128)}, u32[]{:S(2)}) copy-start(f32[2]{0:T(128)} %lambda_ref.1) | copy-start | bytes 28
  59.3 30.6 %copy-start.3 = (f32[128]{0:T(128)S(1)}, f32[128]{0:T(128)}, u32[]{:S(2)}) copy-start(f32[128]{0:T(128)} %param.13) | copy-start | bytes 1540

commit v5 on v4

--- a/solution.py
+++ b/solution.py
@@ -18,7 +18,7 @@
 EMPTY = -1e30
 HIDDEN = -2e38
 BASE2_SCALE = math.log2(math.e) / math.sqrt(QK)
-CASES = ((0, 0, 1), (1, 1, 2), (2, 2, 3), (3, 4, 5), (5, 7, 8), (8, 10, 11), (11, 11, 12))
+CASES = ((0, 0, 1), (1, 2, 3), (3, 4, 5), (5, 7, 8), (8, 10, 11), (11, 11, 12))
 CHUNK = 2
 
 VMEM = pl.BlockSpec(memory_space=pltpu.VMEM)
@@ -52,55 +52,55 @@
 def attend_kernel(place_ref, q_ref, kv_ref, out_ref, v_ref, k0_ref, k1_ref, *scratch):
     z, y = place_ref[0], place_ref[1]
     k_refs = (k0_ref, k1_ref)
-    slots = (scratch[0:2], scratch[2:4])
+    slots = (scratch[0:4], scratch[4:8])
     key_row = lax.broadcasted_iota(jnp.int32, (BLOCK, TILE), 0)
     query_row = lax.rem(lax.broadcasted_iota(jnp.int32, (BLOCK, TILE), 1), BLOCK)
     offsets = key_row - query_row
 
     def step(case, later, slot_later, now, slot_now, peaks):
         low, _, blocks = case
-        if later is not None:
-            queries = both_maps(q_ref, later)
-            tops = [jnp.full((8, TILE), EMPTY, jnp.float32) for _ in range(2)]
-        if now is not None:
-            totals = [jnp.zeros((8, TILE), jnp.float32) for _ in range(2)]
-            summed = [0.0, 0.0]
+        pairs_later = [(b, m) for b in later for m in range(2)]
+        pairs_now = [(b, m) for b in now for m in range(2)]
+        queries = {b: both_maps(q_ref, b) for b in later}
+        tops = {p: jnp.full((8, TILE), EMPTY, jnp.float32) for p in pairs_later}
+        totals = {p: jnp.zeros((8, TILE), jnp.float32) for p in pairs_now}
+        summed = {p: 0.0 for p in pairs_now}
         for first in range(0, blocks, CHUNK):
             last = min(first + CHUNK, blocks)
             rows = slice(first * BLOCK, last * BLOCK)
-            for m in range(2):
-                if later is not None:
+            for at in range(max(len(pairs_later), len(pairs_now))):
+                if at < len(pairs_later):
+                    b, m = pairs_later[at]
                     scores = lax.dot_general(
                         k_refs[m][rows, :],
-                        queries[m],
+                        queries[b][m],
                         (((1,), (1,)), ((), ())),
                         preferred_element_type=jnp.float32,
                     )
                     for block in range(first, last):
                         part = scores[(block - first) * BLOCK : (block - first + 1) * BLOCK]
                         if block >= low:
-                            reach = (z - block) * (Y * BLOCK) + (later - y) * BLOCK
+                            reach = (z - block) * (Y * BLOCK) + (b - y) * BLOCK
                             part = jnp.where(offsets <= reach, part, HIDDEN)
-                        slots[slot_later][m][block * BLOCK : (block + 1) * BLOCK, :] = part
-                        tops[m] = jnp.maximum(tops[m], folded(jnp.max, part))
-                if now is not None:
-                    expo = jnp.exp2(slots[slot_now][m][rows, :] - peaks[m])
-                    totals[m] = totals[m] + folded(jnp.sum, expo)
-                    summed[m] = summed[m] + jnp.dot(
+                        slots[slot_later][at][block * BLOCK : (block + 1) * BLOCK, :] = part
+                        tops[b, m] = jnp.maximum(tops[b, m], folded(jnp.max, part))
+                if at < len(pairs_now):
+                    p = pairs_now[at]
+                    expo = jnp.exp2(slots[slot_now][at][rows, :] - peaks[p])
+                    totals[p] = totals[p] + folded(jnp.sum, expo)
+                    summed[p] = summed[p] + jnp.dot(
                         v_ref[:, rows], expo.astype(jnp.bfloat16), preferred_element_type=jnp.float32
                     )
-        if now is not None:
+        for b in now:
             stats = []
             for m in range(2):
-                total = jnp.sum(totals[m], axis=0, keepdims=True)
+                total = jnp.sum(totals[b, m], axis=0, keepdims=True)
                 total = total.astype(jnp.bfloat16).astype(jnp.float32)
                 inverse = jnp.where(total > 0.0, 1.0 / total, 0.0)
-                out_ref[now, m * VD : (m + 1) * VD, :] = (summed[m] * inverse).astype(jnp.bfloat16)
-                stats += three_parts(peaks[m]) + [total]
-            out_ref[now, 2 * VD :, :] = jnp.concatenate(stats, axis=0).astype(jnp.bfloat16)
-        if later is not None:
-            return [jnp.max(top, axis=0, keepdims=True) for top in tops]
-        return None
+                out_ref[b, m * VD : (m + 1) * VD, :] = (summed[b, m] * inverse).astype(jnp.bfloat16)
+                stats += three_parts(peaks[b, m]) + [total]
+            out_ref[b, 2 * VD :, :] = jnp.concatenate(stats, axis=0).astype(jnp.bfloat16)
+        return {p: jnp.max(top, axis=0, keepdims=True) for p, top in tops.items()}
 
     for case in CASES:
 
@@ -112,13 +112,10 @@
                 k = kv_ref[block, :BLOCK, :]
                 k0_ref[rows, :] = jnp.concatenate([k[:, :QK], k[:, :QK]], axis=1)
                 k1_ref[rows, :] = jnp.concatenate([k[:, QK:], k[:, QK:]], axis=1)
-
-            def two(i, peaks, more=True):
-                odd = step(case, 2 * i + 1, 1, 2 * i, 0, peaks)
-                return step(case, 2 * i + 2 if more else None, 0, 2 * i + 1, 1, odd)
-
-            end = Y // 2 - 1
-            two(end, lax.fori_loop(0, end, two, step(case, 0, 0, None, 1, None)), False)
+            turns = [(), *((b, b + 1) for b in range(0, Y, 2)), ()]
+            peaks = {}
+            for at in range(len(turns) - 1):
+                peaks = step(case, turns[at + 1], at % 2, turns[at], (at + 1) % 2, peaks)
 
 
 def attend(place, queries, key_values):
@@ -130,8 +127,8 @@
         out_specs=VMEM,
         scratch_shapes=[pltpu.VMEM((VD, span), jnp.bfloat16)]
         + [pltpu.VMEM((span, 2 * QK), jnp.bfloat16)] * 2
-        + [pltpu.VMEM((span, TILE), jnp.float32)] * 4,
-        compiler_params=pltpu.CompilerParams(vmem_limit_bytes=16 * 2**20),
+        + [pltpu.VMEM((span, TILE), jnp.float32)] * 8,
+        compiler_params=pltpu.CompilerParams(vmem_limit_bytes=22 * 2**20),
         cost_estimate=pl.CostEstimate(
             flops=4_000_000_000, bytes_accessed=3_000_000, transcendentals=6_000_000
         ),

time: 112 us -> 111 us (level)
  no operation moved by 1% of the time
where the time goes in v5:
time: 111 us
  blocking collectives  101 us (91%)
  Pallas kernels  3.72 us (3%)
  starting transfers between devices  3.62 us (3%)
    all_to_all x1, blocking collectives, body(): parts = lax.all_to_all(parts, 'y', 0, 0, tiled=True)  30.6 us
    all_gather x1, blocking collectives, body(): key_values = lax.all_gather(jnp.concatenate([keys, values], axis=0), 'z')  26.9 us
    all_gather x1, blocking collectives, body(): rows = lax.all_gather(tokens, 'tp', axis=0, tiled=True)  23.7 us
    all_to_all x1, blocking collectives, body(): lax.all_to_all(partial_rows.reshape(tp, -1, partial_rows.shape[1]), 'tp',...  19.5 us
    all_to_all x1, starting transfers between devices, to_everyone(): lax.all_to_all(jnp.broadcast_to(value[None], (length, *value.shape)), axi...  3.62 us
    pallas_call x1, Pallas kernels, attend(): pl.pallas_call(attend_kernel, out_shape=jax.ShapeDtypeStruct((Y, SEND_ROW...  2.52 us
  transfers between devices with their start and end apart: 1, of which 0 were waited for; matrix products, arithmetic and copies ran while one was open for 1% of the time, Pallas kernels for 0%

profile of v5, /device:TPU:1, one launch (start us, length us, event | category | flops | bytes accessed | tf_op | source)
XLA Modules:
  0.0 110.8 jit_solution(12012191444279675847)
XLA Ops:
  0.0 0.0 copy-start
  0.0 23.7 %all_gather.9 = bf16[128,2048]{1,0:T(8,128)(2,1)S(1)} all-gather(bf16[16,2048]{1,0:T(8,128)(2,1)} %param.7), channel_id=1, replica_groups=mesh['z'=12,'y'=8,'tp'=8] {'tp'}, dimensions={0}, use_global_device_ids=true | all-gather | bytes 589824 | tf_op jit(solution)/shard_map/all_gather | solution.py:189
  23.8 0.0 copy-done
  23.8 0.3 convolution_convert_fusion
  24.1 0.0 copy-start.4
  24.1 0.8 broadcast_in_dim.2
  24.9 3.6 %all-to-all-start = ((bf16[8,128,256]{2,1,0:T(8,128)(2,1)}), bf16[8,128,256]{2,1,0:T(8,128)(2,1)S(1)}, u32[]{:S(2)}, u32[]{:S(2)}) async-start(bf16[8,128,256]{2,1,0:T(8,128)(2,1)} %broadcast_in_dim.2), calls=%async_computation | async-start | bytes 1048576 | tf_op jit(solution)/shard_map/all_to_all | solution.py:182
  28.5 0.1 pad_add_fusion.place_ref
  28.6 0.0 copy-done.4
  28.6 0.4 convolution_convert_fusion.1
  29.0 0.0 copy-done.5
  29.0 0.3 convolution_convert_fusion.2
  29.3 26.9 %all-gather = bf16[3072,128]{1,0:T(8,128)(2,1)S(1)} all-gather(bf16[256,128]{1,0:T(8,128)(2,1)S(1)} %pad_maximum_fusion), channel_id=2, replica_groups=mesh['z'=12,'y'=8,'tp'=8] {'z'}, dimensions={0}, use_global_device_ids=true | all-gather | bytes 851968 | tf_op jit(solution)/shard_map/all_gather | solution.py:195
  56.2 0.0 all-to-all-done.q_ref
  56.2 2.5 %attend.1 = bf16[8,264,256]{2,1,0:T(8,128)(2,1)S(1)} custom-call(s32[2]{0:T(128)S(1)} %pad_add_fusion.place_ref, bf16[8,128,256]{2,1,0:T(8,128)(2,1)S(1)} %all-to-all-done.q_ref, bf16[12,256,128]{2,1,0:T(8,128)(2,1)S(1)} %bitcast.11), custom_call_target="tpu_custom_call" | custom-call | flops 4000000000 | bytes 3000000 | tf_op jit(solution)/shard_map/attend/pallas_call | solution.py:123
  58.8 0.0 copy-start.1
  58.8 0.0 copy-start.2
  58.8 0.0 copy-start.3
  58.8 30.6 %all_to_all.15.part_ref = bf16[8,264,256]{2,1,0:T(8,128)(2,1)S(1)} all-to-all(bf16[8,264,256]{2,1,0:T(8,128)(2,1)S(1)} %attend.1), channel_id=1, replica_groups=mesh['z'=12,'y'=8,'tp'=8] {'y'}, dimensions={0} | all-to-all | bytes 2162688 | tf_op jit(solution)/shard_map/all_to_all | solution.py:198
  89.4 0.0 copy-done.1
  89.4 0.0 copy-done.2
  89.4 1.2 %merge.1 = bf16[128,2048]{1,0:T(8,128)(2,1)S(1)} custom-call(bf16[8,264,256]{2,1,0:T(8,128)(2,1)S(1)} %all_to_all.15.part_ref, f32[2]{0:T(128)S(1)} %copy-done.2, f32[1,128]{1,0:T(1,128)S(1)} %bitcast.13, bf16[256,2048]{1,0:T(8,128)(2,1)S(1)} %copy-done.1), custom_call_target="tpu_custom_call" | custom-call | flops 1000000000 | bytes 3000000 | tf_op jit(solution)/shard_map/merge/pallas_call | solution.py:167
  90.6 19.5 %all_to_all.16 = bf16[8,16,2048]{2,1,0:T(8,128)(2,1)S(1)} all-to-all(bf16[8,16,2048]{2,1,0:T(8,128)(2,1)S(1)} %bitcast.12), channel_id=1, replica_groups=mesh['z'=12,'y'=8,'tp'=8] {'tp'}, dimensions={0} | all-to-all | bytes 1048576 | tf_op jit(solution)/shard_map/all_to_all | solution.py:200
  110.1 0.7 reduce_sum.12
  (3 shorter events, 0.0 us)
Async XLA Ops:
  0.0 23.8 %copy-start = (bf16[2048,256]{1,0:T(8,128)(2,1)S(1)}, bf16[2048,256]{1,0:T(8,128)(2,1)}, u32[]{:S(2)}) copy-start(bf16[2048,256]{1,0:T(8,128)(2,1)} %param.8) | copy-start | bytes 3145732
  24.1 4.6 %copy-start.4 = (bf16[2048,128]{1,0:T(8,128)(2,1)S(1)}, bf16[2048,128]{1,0:T(8,128)(2,1)}, u32[]{:S(2)}) copy-start(bf16[2048,128]{1,0:T(8,128)(2,1)} %param.10) | copy-start | bytes 1572868
  24.9 4.1 %copy-start.5 = (bf16[2048,128]{1,0:T(8,128)(2,1)S(1)}, bf16[2048,128]{1,0:T(8,128)(2,1)}, u32[]{:S(2)}) copy-start(bf16[2048,128]{1,0:T(8,128)(2,1)} %param.9) | copy-start | bytes 1572868
  24.9 31.3 %all-to-all-start = ((bf16[8,128,256]{2,1,0:T(8,128)(2,1)}), bf16[8,128,256]{2,1,0:T(8,128)(2,1)S(1)}, u32[]{:S(2)}, u32[]{:S(2)}) async-start(bf16[8,128,256]{2,1,0:T(8,128)(2,1)} %broadcast_in_dim.2), calls=%async_computation | async-start | bytes 1048576 | tf_op jit(solution)/shard_map/all_to_all | solution.py:182
  58.8 30.6 %copy-start.1 = (bf16[256,2048]{1,0:T(8,128)(2,1)S(1)}, bf16[256,2048]{1,0:T(8,128)(2,1)}, u32[]{:S(2)}) copy-start(bf16[256,2048]{1,0:T(8,128)(2,1)} %w_ref.1) | copy-start | bytes 3145732
  58.8 30.6 %copy-start.2 = (f32[2]{0:T(128)S(1)}, f32[2]{0:T(128)}, u32[]{:S(2)}) copy-start(f32[2]{0:T(128)} %lambda_ref.1) | copy-start | bytes 28
  58.8 30.6 %copy-start.3 = (f32[128]{0:T(128)S(1)}, f32[128]{0:T(128)}, u32[]{:S(2)}) copy-start(f32[128]{0:T(128)} %param.13) | copy-start | bytes 1540

commit v6 on v5

--- a/solution.py
+++ b/solution.py
@@ -177,6 +177,24 @@
     )(parts, lambda_head, sub_gain.reshape(1, VD), w_out)
 
 
+def sum_kernel(part_ref, out_ref):
+    total = part_ref[0].astype(jnp.float32)
+    for n in range(1, part_ref.shape[0]):
+        total = total + part_ref[n].astype(jnp.float32)
+    out_ref[...] = total.astype(jnp.bfloat16)
+
+
+def summed_rows(parts):
+    return pl.pallas_call(
+        sum_kernel,
+        out_shape=jax.ShapeDtypeStruct(parts.shape[1:], jnp.bfloat16),
+        in_specs=[VMEM],
+        out_specs=VMEM,
+        compiler_params=pltpu.CompilerParams(vmem_limit_bytes=4 * 2**20),
+        name="sum_rows",
+    )(parts)
+
+
 def to_everyone(value, axis):
     length = lax.axis_size(axis)
     return lax.all_to_all(
@@ -200,7 +218,7 @@
     arrived = lax.all_to_all(
         partial_rows.reshape(tp, -1, partial_rows.shape[1]), "tp", 0, 0, tiled=True
     )
-    return arrived.astype(jnp.float32).sum(axis=0).astype(jnp.bfloat16)
+    return summed_rows(arrived)
 
 
 def solution(mesh):

time: 111 us -> 111 us (level)
  no operation moved by 1% of the time
where the time goes in v6:
time: 111 us
  blocking collectives  101 us (91%)
  Pallas kernels  4.42 us (4%)
  starting transfers between devices  3.62 us (3%)
    all_to_all x1, blocking collectives, body(): parts = lax.all_to_all(parts, 'y', 0, 0, tiled=True)  30.6 us
    all_gather x1, blocking collectives, body(): key_values = lax.all_gather(jnp.concatenate([keys, values], axis=0), 'z')  26.9 us
    all_gather x1, blocking collectives, body(): rows = lax.all_gather(tokens, 'tp', axis=0, tiled=True)  23.7 us
    all_to_all x1, blocking collectives, body(): lax.all_to_all(partial_rows.reshape(tp, -1, partial_rows.shape[1]), 'tp',...  19.5 us
    all_to_all x1, starting transfers between devices, to_everyone(): lax.all_to_all(jnp.broadcast_to(value[None], (length, *value.shape)), axi...  3.62 us
    pallas_call x1, Pallas kernels, attend(): pl.pallas_call(attend_kernel, out_shape=jax.ShapeDtypeStruct((Y, SEND_ROW...  2.52 us
  transfers between devices with their start and end apart: 1, of which 0 were waited for; matrix products, arithmetic and copies ran while one was open for 1% of the time, Pallas kernels for 0%

profile of v6, /device:TPU:1, one launch (start us, length us, event | category | flops | bytes accessed | tf_op | source)
XLA Modules:
  0.0 110.8 jit_solution(1230373597155395872)
XLA Ops:
  0.0 0.0 copy-start
  0.0 23.7 %all_gather.9 = bf16[128,2048]{1,0:T(8,128)(2,1)S(1)} all-gather(bf16[16,2048]{1,0:T(8,128)(2,1)} %param.7), channel_id=1, replica_groups=mesh['z'=12,'y'=8,'tp'=8] {'tp'}, dimensions={0}, use_global_device_ids=true | all-gather | bytes 589824 | tf_op jit(solution)/shard_map/all_gather | solution.py:207
  23.8 0.0 copy-done
  23.8 0.3 convolution_convert_fusion
  24.1 0.0 copy-start.4
  24.1 0.8 broadcast_in_dim.2
  24.9 3.6 %all-to-all-start = ((bf16[8,128,256]{2,1,0:T(8,128)(2,1)}), bf16[8,128,256]{2,1,0:T(8,128)(2,1)S(1)}, u32[]{:S(2)}, u32[]{:S(2)}) async-start(bf16[8,128,256]{2,1,0:T(8,128)(2,1)} %broadcast_in_dim.2), calls=%async_computation | async-start | bytes 1048576 | tf_op jit(solution)/shard_map/all_to_all | solution.py:200
  28.6 0.1 pad_add_fusion.place_ref
  28.6 0.0 copy-done.4
  28.6 0.4 convolution_convert_fusion.1
  29.0 0.0 copy-done.5
  29.0 0.3 convolution_convert_fusion.2
  29.3 26.9 %all-gather = bf16[3072,128]{1,0:T(8,128)(2,1)S(1)} all-gather(bf16[256,128]{1,0:T(8,128)(2,1)S(1)} %pad_maximum_fusion), channel_id=2, replica_groups=mesh['z'=12,'y'=8,'tp'=8] {'z'}, dimensions={0}, use_global_device_ids=true | all-gather | bytes 851968 | tf_op jit(solution)/shard_map/all_gather | solution.py:213
  56.2 0.0 all-to-all-done.q_ref
  56.2 2.5 %attend.1 = bf16[8,264,256]{2,1,0:T(8,128)(2,1)S(1)} custom-call(s32[2]{0:T(128)S(1)} %pad_add_fusion.place_ref, bf16[8,128,256]{2,1,0:T(8,128)(2,1)S(1)} %all-to-all-done.q_ref, bf16[12,256,128]{2,1,0:T(8,128)(2,1)S(1)} %bitcast.11), custom_call_target="tpu_custom_call" | custom-call | flops 4000000000 | bytes 3000000 | tf_op jit(solution)/shard_map/attend/pallas_call | solution.py:123
  58.8 0.0 copy-start.1
  58.8 0.0 copy-start.2
  58.8 0.0 copy-start.3
  58.8 30.6 %all_to_all.15.part_ref = bf16[8,264,256]{2,1,0:T(8,128)(2,1)S(1)} all-to-all(bf16[8,264,256]{2,1,0:T(8,128)(2,1)S(1)} %attend.1), channel_id=1, replica_groups=mesh['z'=12,'y'=8,'tp'=8] {'y'}, dimensions={0} | all-to-all | bytes 2162688 | tf_op jit(solution)/shard_map/all_to_all | solution.py:216
  89.4 0.0 copy-done.1
  89.4 0.0 copy-done.3
  89.4 1.2 %merge.1 = bf16[128,2048]{1,0:T(8,128)(2,1)S(1)} custom-call(bf16[8,264,256]{2,1,0:T(8,128)(2,1)S(1)} %all_to_all.15.part_ref, f32[2]{0:T(128)S(1)} %copy-done.2, f32[1,128]{1,0:T(1,128)S(1)} %bitcast.13, bf16[256,2048]{1,0:T(8,128)(2,1)S(1)} %copy-done.1), custom_call_target="tpu_custom_call" | custom-call | flops 1000000000 | bytes 3000000 | tf_op jit(solution)/shard_map/merge/pallas_call | solution.py:167
  90.6 19.5 %all_to_all.16.part_ref = bf16[8,16,2048]{2,1,0:T(8,128)(2,1)S(1)} all-to-all(bf16[8,16,2048]{2,1,0:T(8,128)(2,1)S(1)} %bitcast.12), channel_id=1, replica_groups=mesh['z'=12,'y'=8,'tp'=8] {'tp'}, dimensions={0} | all-to-all | bytes 1048576 | tf_op jit(solution)/shard_map/all_to_all | solution.py:218
  110.1 0.7 sum_rows.1
  (3 shorter events, 0.0 us)
Async XLA Ops:
  0.0 23.8 %copy-start = (bf16[2048,256]{1,0:T(8,128)(2,1)S(1)}, bf16[2048,256]{1,0:T(8,128)(2,1)}, u32[]{:S(2)}) copy-start(bf16[2048,256]{1,0:T(8,128)(2,1)} %param.8) | copy-start | bytes 3145732
  24.1 4.6 %copy-start.4 = (bf16[2048,128]{1,0:T(8,128)(2,1)S(1)}, bf16[2048,128]{1,0:T(8,128)(2,1)}, u32[]{:S(2)}) copy-start(bf16[2048,128]{1,0:T(8,128)(2,1)} %param.10) | copy-start | bytes 1572868
  24.9 4.1 %copy-start.5 = (bf16[2048,128]{1,0:T(8,128)(2,1)S(1)}, bf16[2048,128]{1,0:T(8,128)(2,1)}, u32[]{:S(2)}) copy-start(bf16[2048,128]{1,0:T(8,128)(2,1)} %param.9) | copy-start | bytes 1572868
  24.9 31.3 %all-to-all-start = ((bf16[8,128,256]{2,1,0:T(8,128)(2,1)}), bf16[8,128,256]{2,1,0:T(8,128)(2,1)S(1)}, u32[]{:S(2)}, u32[]{:S(2)}) async-start(bf16[8,128,256]{2,1,0:T(8,128)(2,1)} %broadcast_in_dim.2), calls=%async_computation | async-start | bytes 1048576 | tf_op jit(solution)/shard_map/all_to_all | solution.py:200
  58.8 30.6 %copy-start.1 = (bf16[256,2048]{1,0:T(8,128)(2,1)S(1)}, bf16[256,2048]{1,0:T(8,128)(2,1)}, u32[]{:S(2)}) copy-start(bf16[256,2048]{1,0:T(8,128)(2,1)} %w_ref.1) | copy-start | bytes 3145732
  58.8 30.6 %copy-start.2 = (f32[2]{0:T(128)S(1)}, f32[2]{0:T(128)}, u32[]{:S(2)}) copy-start(f32[2]{0:T(128)} %lambda_ref.1) | copy-start | bytes 28
  58.8 30.6 %copy-start.3 = (f32[128]{0:T(128)S(1)}, f32[128]{0:T(128)}, u32[]{:S(2)}) copy-start(f32[128]{0:T(128)} %param.13) | copy-start | bytes 1540
